TPU v7x, 256 devices: a whole 4x4x8 slice. The times are simulated.
256 devices in a mesh: sp: 64 (over z, x, core), tp: 4 (over y).
Axes of the slice: x: 4, y: 4, z: 8, core: 2. Of those that a mesh axis runs over, the one named last changes fastest.
Arguments:
- residual: bfloat16 [16384, 2048], P(('sp', 'tp')), may hold values from -6 to 6
- query_vectors: bfloat16 [16384, 512], P('sp', 'tp'), may hold values from -6 to 6
- key_vectors: bfloat16 [16384, 512], P('sp', 'tp'), may hold values from -6 to 6
- value_vectors: bfloat16 [16384, 512], P('sp', 'tp'), may hold values from -6 to 6
- in_gate: float32 [8, 16384], P('tp', 'sp'), may hold values from -9 to 190
- forget_gate: float32 [8, 16384], P('tp', 'sp'), may hold values from -1 to 12
- documents: int32 [16384], P('sp'), may hold values from 0 to 15, never falling along the last dimension, each value on 1 to 2048 neighbouring positions
- w_out: bfloat16 [512, 2048], P('tp'), may hold values from -0.25 to 0.25
- norm_gain: bfloat16 [2048], replicated, may hold values from 0.099609375 to 1.8984375
- w_up: bfloat16 [2048, 8192], P('sp', 'tp'), may hold values from -0.125 to 0.125
- w_down: bfloat16 [8192, 2048], P('tp', 'sp'), may hold values from -0.0625 to 0.0625
Outputs:
- layer_out: bfloat16 [16384, 2048], P(('sp', 'tp'))
Inputs may be any that keep to these rules, and one draw needn't show every extreme that they name: `documents`: document numbers never fall along the positions; every document has 1 to 2048 positions.
All inputs are finite; a program needn't handle non-finite values.
Results may differ from a plain program's by a relative error of at most 0.015.
Values may be sent and summed in bfloat16 or wider, within the bound.
No kernel may reach another device: no remote copies, remote signals or barrier semaphores. Data moves between devices by JAX's collectives and lax.ppermute only.
A program may use at most 64 MiB of HBM per device.

v0:
```python
import functools

import jax
import jax.numpy as jnp
from jax import lax
from jax.experimental import pallas as pl
from jax.experimental.pallas import tpu as pltpu
from jax.sharding import Mesh
from jax.sharding import PartitionSpec as P


SP = ("sp_0", "sp_1", "sp_2")
SP_TP = ("sp_0", "sp_1", "sp_2", "tp")
Z, X, C, Y = SP_TP
CHIPS_BACK = 4
very_negative = -1e30
epsilon = 1e-06
f32 = jnp.float32
bf16 = jnp.bfloat16
HIGH = lax.Precision.HIGHEST

VM = pl.BlockSpec(memory_space=pltpu.VMEM)
SM = pl.BlockSpec(memory_space=pltpu.SMEM)
ANY = pl.BlockSpec(memory_space=pl.ANY)
HBM = pl.BlockSpec(memory_space=pltpu.HBM)


def call(kernel, outs, ins, args, scratch=(), flops=1, traffic=1, vmem=16):
    many = isinstance(outs, (list, tuple))
    return pl.pallas_call(
        kernel,
        out_shape=outs,
        in_specs=ins,
        out_specs=[VM] * len(outs) if many else VM,
        scratch_shapes=list(scratch),
        cost_estimate=pl.CostEstimate(flops=flops, bytes_accessed=traffic, transcendentals=0),
        compiler_params=pltpu.CompilerParams(vmem_limit_bytes=vmem * 1024 * 1024),
    )(*args)


def halves(shape, zero, one):
    lane = lax.broadcasted_iota(jnp.int32, shape, 1)
    return jnp.where(lane < 64, zero, one)


def copy_all(pairs, sems):
    copies = [pltpu.make_async_copy(a, b, sems.at[k]) for k, (a, b) in enumerate(pairs)]
    for c in copies:
        c.start()
    for c in copies:
        c.wait()


def at(start, size):
    return pl.ds(pl.multiple_of(start, size), size)


STATE_ROWS = 72


def memory_kernel(*refs):
    state, packed = refs[6:8]
    in_gate, forget_gate, docs, queries, keys, values = refs[8:14]
    copy_all(list(zip(refs[:6], refs[8:14])), refs[14])
    forget = forget_gate[...]
    decay = jnp.minimum(forget, 0.0) - jnp.log1p(jnp.exp(-jnp.abs(forget)))
    lane = lax.broadcasted_iota(jnp.int32, decay.shape, 1)
    total = decay
    step = 1
    while step < decay.shape[1]:
        total = total + jnp.where(lane >= step, pltpu.roll(total, step, 1), 0.0)
        step *= 2
    gate = in_gate[...]
    doc = docs[...].astype(f32)
    table = jnp.concatenate([total, gate, doc, jnp.zeros((3, doc.shape[1]), f32)], axis=0)
    turned = jnp.transpose(table)
    last = doc[:, -1:]
    end = total[:, -1:]
    growth = jnp.where(doc == last, end - total + gate, very_negative)
    top = jnp.max(growth, axis=1, keepdims=True)
    latest = turned[:, 4:5] == last
    weight = []
    for h in range(2):
        grown = jnp.where(latest, end[h:h + 1] - turned[:, h:h + 1] + turned[:, 2 + h:3 + h], very_negative)
        weight.append(jnp.exp(grown - top[h:h + 1]))
    wide = halves(keys.shape, weight[0], weight[1])
    weighted = wide * keys[...].astype(f32)
    full = jnp.dot(jnp.transpose(weighted), values[...].astype(f32), precision=HIGH, preferred_element_type=f32)
    state[0:64, :] = halves((64, 128), full[0:64], full[64:128])
    normal = jnp.sum(weighted, axis=0, keepdims=True)
    tail = [
        normal,
        halves((1, 128), top[0:1], top[1:2]),
        halves((1, 128), end[0:1], end[1:2]),
        jnp.broadcast_to(last, (1, 128)),
        jnp.zeros((4, 128), f32),
    ]
    state[64:72, :] = jnp.concatenate(tail, axis=0)

    length = queries.shape[0]
    scaled = queries[...] * jnp.asarray(0.125, bf16)
    key = keys[...]
    value = values[...]
    row_ids = lax.broadcasted_iota(jnp.int32, (length, length), 0)
    col_ids = lax.broadcasted_iota(jnp.int32, (length, length), 1)
    allowed = (col_ids <= row_ids) & (turned[:, 4:5] == doc)
    found = []
    for h in range(2):
        inside = jnp.where(
            allowed,
            turned[:, h:h + 1] - total[h:h + 1, :] + gate[h:h + 1, :],
            very_negative,
        )
        peak = jnp.max(inside, axis=1, keepdims=True)
        mine = halves(key.shape, jnp.asarray(1 - h, bf16), jnp.asarray(h, bf16)) * key
        scores = lax.dot_general(scaled, mine, (((1,), (1,)), ((), ())), preferred_element_type=f32)
        weight = jnp.exp(inside - peak) * scores
        summed = jnp.dot(weight.astype(bf16), value, preferred_element_type=f32)
        found.append((summed, jnp.sum(weight, axis=1, keepdims=True), peak, turned[:, h:h + 1]))
    for k in range(4):
        packed[:, k * 128:k * 128 + 128] = halves((length, 128), found[0][k], found[1][k])
    packed[:, 512:640] = jnp.broadcast_to(turned[:, 4:5], (length, 128))
    packed[:, 640:768] = scaled.astype(f32)


def merge_kernel(packed, states_own, other, mixed):
    numer, denom, inner, moved, doc, scaled = (packed[:, k * 128:k * 128 + 128] for k in range(6))
    c = lax.axis_index(C)
    chip = lax.axis_index(Z) * 4 + lax.axis_index(X)
    upper = jnp.zeros((1, 128), jnp.int32) + c == 1
    chips = jnp.zeros((1, 128), jnp.int32) + chip
    states = [(other[0:STATE_ROWS], upper)]
    for back in range(1, CHIPS_BACK + 1):
        there = slice(back * STATE_ROWS, (back + 1) * STATE_ROWS)
        mine, theirs = states_own[there], other[there]
        states.append((jnp.where(c == 1, mine, theirs), chips >= back))
        states.append((jnp.where(c == 1, theirs, mine), chips >= back))
    open_doc = jnp.where(upper, states[0][0][67:68], states[1][0][67:68])
    decayed = jnp.zeros((1, 128), f32)
    reach = []
    for state, there in states:
        joined = (state[67:68] == open_doc) & there
        reach.append(jnp.where(joined, state[65:66] + decayed, very_negative))
        decayed = decayed + jnp.where(there, state[66:67], 0.0)
    top = functools.reduce(jnp.maximum, reach)
    memory = jnp.zeros((64, 128), f32)
    normal = jnp.zeros((1, 128), f32)
    for far, (state, _) in zip(reach, states):
        scale = jnp.where(far > 0.5 * very_negative, jnp.exp(far - top), 0.0)
        memory = memory + scale * state[0:64]
        normal = normal + scale * state[64:65]
    open_here = (doc == open_doc) & (top > 0.5 * very_negative)
    outside = jnp.where(open_here, moved + top, very_negative)
    both = jnp.maximum(outside, inner)
    carried = jnp.exp(outside - both)
    kept = jnp.exp(inner - both)
    blocks = jnp.concatenate([halves((64, 128), memory, 0.0), halves((64, 128), 0.0, memory)], axis=0)
    readout = jnp.dot(scaled, blocks, precision=HIGH, preferred_element_type=f32)
    ones = jnp.concatenate([halves((64, 128), 1.0, 0.0), halves((64, 128), 0.0, 1.0)], axis=0)
    along = jnp.dot(scaled * normal, ones, precision=HIGH, preferred_element_type=f32)
    top_part = kept * numer + carried * readout
    low_part = kept * denom + carried * along
    result = (top_part / jnp.maximum(jnp.abs(low_part), jnp.exp(-both))).astype(bf16)
    mixed[...] = result


def early_kernel(residual, w_out, out, sems):
    rows = at(lax.axis_index(C) * 64, 64)
    copy_all(
        [(residual, out.at[k, 0:64]) for k in range(4)]
        + [(w_out.at[rows], out.at[k, 64:128]) for k in range(4)],
        sems,
    )


def middle_kernel(early_own, early_other, gain, mixes_own, mixes_other, middle, normed, weights, heads, projected):
    c, y = lax.axis_index(C), lax.axis_index(Y)
    for core, early in ((0, early_own), (1, early_other)):
        for there in range(4):
            row = at(there * 128 + (c + core) % 2 * 64, 64)
            weights[row, :] = early[there, 64:128, :]
    for core, mixes in ((0, mixes_own), (1, mixes_other)):
        for back in range(4):
            lanes = at((y + 4 - back) % 4 * 128, 128)
            for k in range(4):
                row = (core * 4 + k) * 64
                heads[row:row + 64, lanes] = mixes[at(back * 256 + (y + k) % 4 * 64, 64), :]

    def columns(n, carry):
        part = at(n * 256, 256)
        projected[:, part] = jnp.dot(heads[...], weights[:, part], preferred_element_type=f32)
        return carry

    lax.fori_loop(0, 8, columns, 0, unroll=2)
    for core, early in ((0, early_own), (1, early_other)):
        def rows(k, carry, core=core, early=early):
            part = at((core * 4 + k) * 64, 64)
            kept = early[(y + k) % 4, 0:64, :]
            mid = (kept.astype(f32) + projected[part, :]).astype(bf16)
            middle[part, :] = mid
            wide = mid.astype(f32)
            factor = lax.rsqrt(jnp.mean(wide * wide, axis=1, keepdims=True) + epsilon)
            normed[part, :] = (wide * factor * gain[...].astype(f32)).astype(bf16)
            return carry

        lax.fori_loop(0, 4, rows, 0, unroll=2)


OFFSETS = (0, -1, 1, -2, 2, -3, 3, -4)
X_OFFSETS = (0, -1, 1, 2)


def up_kernel(slots, final, normed, *refs):
    if final:
        units, (before, out, weights) = refs[:2], refs[2:]
    else:
        units, (out, weights) = refs[:len(slots)], refs[len(slots):]
    z, x = lax.axis_index(Z), lax.axis_index(X)
    for j, slot in enumerate(slots):
        chunk = 0 if final else (z + 8 + OFFSETS[slot]) % 8
        for k, offset in enumerate(X_OFFSETS):
            row = at(chunk * 256 + (x + 4 + offset) % 4 * 64, 64)
            unit, start = (units[k // 2], k % 2 * 64) if final else (units[j], k * 64)
            weights[row, :] = unit[start:start + 64, :]
    if final:
        lanes = at((z + 8 + OFFSETS[slots[0]]) % 8 * 256, 256)
    else:
        missing = at((z + 8 + OFFSETS[7]) % 8 * 256, 256)
        weights[missing, :] = jnp.zeros((256, 1024), bf16)

    def columns(n, carry):
        part = at(n * 256, 256)
        if final:
            term = before[:, part] + jnp.dot(normed[:, lanes], weights[:, part], preferred_element_type=f32)
            positive = jnp.maximum(term, 0.0)
            out[:, part] = (positive * positive).astype(bf16)
        else:
            out[:, part] = jnp.dot(normed[...], weights[:, part], preferred_element_type=f32)
        return carry

    lax.fori_loop(0, 4, columns, 0)


def gather_kernel(rows, *refs):
    pieces, out, sems = refs[:-2], refs[-2], refs[-1]
    copy_all([(p, out.at[k * rows:(k + 1) * rows]) for k, p in enumerate(pieces)], sems)


def down_kernel(other_half, hidden, mine, before, after, far_a, far_b, *refs):
    if other_half:
        partial, outs, weights, ordered = refs[0], refs[1:9], refs[9], refs[10]
        ordered[0:256, :] = hidden[256:512, :]
        ordered[256:512, :] = hidden[0:256, :]
    else:
        out, weights = refs
        ordered = hidden
    c, z, x = lax.axis_index(C), lax.axis_index(Z), lax.axis_index(X)
    lanes = at((1 - c if other_half else c) * 1024, 1024)
    for slot in range(8):
        there = (z + 8 + OFFSETS[slot]) % 8 * 128
        far, row = (far_a, slot * 32) if slot < 4 else (far_b, slot * 32 - 128)
        weights[at(there + (x + 2) % 4 * 32, 32), :] = far[row:row + 32, lanes]
        for source, offset in ((mine, 0), (before, -1), (after, 1)):
            to = at(there + (x + 4 + offset) % 4 * 32, 32)
            weights[to, :] = source[slot * 32:slot * 32 + 32, lanes]

    def columns(n, carry):
        part = at(n * 256, 256)
        terms = lax.dot_general(
            ordered[...], weights[part, :], (((1,), (1,)), ((), ())), preferred_element_type=f32
        )
        if other_half:
            terms = (terms + partial[:, part]).astype(bf16)
            for k in range(8):
                outs[k][:, part] = terms[k * 64:k * 64 + 64]
        else:
            out[:, part] = terms
        return carry

    lax.fori_loop(0, 4, columns, 0)


def last_kernel(middle, *refs):
    terms, (out, stacked) = refs[:8], refs[8:]
    c = lax.axis_index(C)
    for core in range(2):
        lanes = at((c + core) % 2 * 256, 256)
        for k in range(4):
            for b in range(4):
                row = (b * 4 + k) * 64
                stacked[row:row + 64, lanes] = terms[core * 4 + k][:, b * 256:b * 256 + 256]
    s = lax.broadcasted_iota(jnp.int32, (512, 512), 0)
    d = lax.broadcasted_iota(jnp.int32, (512, 512), 1)
    wanted = ((s % 256) // 32) * 64 + (s // 256) * 32 + s % 32
    turn = (wanted == d).astype(f32).astype(bf16)
    for b in range(4):
        spread = jnp.dot(stacked[b * 256:b * 256 + 256, :], turn, preferred_element_type=f32)
        summed = spread[0:64] + spread[64:128] + spread[128:192] + spread[192:256]
        part = slice(b * 512, b * 512 + 512)
        out[:, part] = (middle[0:64, part].astype(f32) + summed).astype(bf16)


def shift(value, axis, by):
    n = lax.axis_size(axis)
    return lax.ppermute(value, axis, [(i, (i + by) % n) for i in range(n)])


def to_peer(value, core, by):
    pairs = [(c * 4 + y, (c ^ core) * 4 + (y + by) % 4) for c in range(2) for y in range(4)]
    return lax.ppermute(value, (C, Y), pairs)


def z_ring(piece, steps=4):
    up, down = [piece], [piece]
    for step in range(steps):
        up.append(shift(up[-1], Z, 1))
        if step < 3:
            down.append(shift(down[-1], Z, -1))
    return [piece, up[1], down[1], up[2], down[2], up[3], down[3], *up[4:]]


def half_kernel(one, two, first, second, sems):
    rows = first.shape[0]
    copy_all([(one.at[0:rows], first), (two.at[rows:2 * rows], second)], sems)


def half_of_each(one, two):
    half = jax.ShapeDtypeStruct((one.shape[0] // 2, one.shape[1]), one.dtype)
    return call(
        half_kernel,
        [half, half],
        [ANY] * 2,
        (one, two),
        scratch=[pltpu.SemaphoreType.DMA((2,))],
        flops=1_000_000,
        vmem=4,
    )


def layer(
    residual,
    query_vectors,
    key_vectors,
    value_vectors,
    in_gate,
    forget_gate,
    documents,
    w_out,
    norm_gain,
    w_up,
    w_down,
):
    c = lax.axis_index(C)
    first = c == 0
    left, right = w_up[:, :1024], w_up[:, 1024:]
    keep, give = jnp.where(first, left, right), jnp.where(first, right, left)
    taken = shift(give, C, 1)
    mine = jnp.where(
        first, jnp.concatenate([keep, taken], axis=0), jnp.concatenate([taken, keep], axis=0)
    )
    across = [mine, shift(mine, X, 1), shift(mine, X, -1), shift(mine, X, 2)]
    unit = call(
        functools.partial(gather_kernel, 64),
        jax.ShapeDtypeStruct((256, 1024), bf16),
        [ANY] * 4,
        across,
        scratch=[pltpu.SemaphoreType.DMA((4,))],
        flops=1_000_000,
        vmem=4,
    )
    up_units = z_ring(unit, 3)
    far_up, far_down = half_of_each(up_units[5], up_units[6])
    far_up, far_down = shift(far_up, Z, 1), shift(far_down, Z, -1)
    down_columns = call(
        functools.partial(gather_kernel, 32),
        jax.ShapeDtypeStruct((256, 2048), bf16),
        [ANY] * 8,
        z_ring(w_down.T),
        scratch=[pltpu.SemaphoreType.DMA((8,))],
        flops=1_000_000,
        vmem=4,
    )
    before, after = shift(down_columns, X, 1), shift(down_columns, X, -1)
    far_a, far_b = half_of_each(before, after)
    far_a, far_b = shift(far_a, X, 1), shift(far_b, X, -1)
    docs = documents.reshape(1, -1)
    tokens = query_vectors.shape[0]
    pair = pltpu.VMEM((tokens, 128), bf16)
    state, packed = call(
        memory_kernel,
        [
            jax.ShapeDtypeStruct((STATE_ROWS, 128), f32),
            jax.ShapeDtypeStruct((tokens, 768), f32),
        ],
        [HBM] * 6,
        (in_gate, forget_gate, docs, query_vectors, key_vectors, value_vectors),
        scratch=[
            pltpu.VMEM(in_gate.shape, f32),
            pltpu.VMEM(in_gate.shape, f32),
            pltpu.VMEM(docs.shape, jnp.int32),
            pair,
            pair,
            pair,
            pltpu.SemaphoreType.DMA((6,)),
        ],
        flops=150_000_000,
    )
    received = [
        lax.ppermute(state, (Z, X), [(i, (i + back) % 32) for i in range(32)])
        for back in range(1, CHIPS_BACK + 1)
    ]
    states = call(
        functools.partial(gather_kernel, STATE_ROWS),
        jax.ShapeDtypeStruct((STATE_ROWS * (CHIPS_BACK + 1), 128), f32),
        [ANY] * (CHIPS_BACK + 1),
        (state, *received),
        scratch=[pltpu.SemaphoreType.DMA((CHIPS_BACK + 1,))],
        flops=1_000_000,
        vmem=4,
    )
    other = shift(states, C, 1)
    early = call(
        early_kernel,
        jax.ShapeDtypeStruct((4, 128, 2048), bf16),
        [HBM] * 2,
        (residual, w_out),
        scratch=[pltpu.SemaphoreType.DMA((8,))],
        flops=1_000_000,
        vmem=4,
    )
    early_own = lax.all_to_all(early, Y, 0, 0, tiled=True)
    early_other = shift(early_own, C, 1)
    mixed = call(
        merge_kernel,
        jax.ShapeDtypeStruct((tokens, 128), bf16),
        [VM] * 3,
        (packed, states, other),
        flops=100_000_000,
    )
    peers = [(core, by) for core in range(2) for by in range(4)]
    mixes = call(
        functools.partial(gather_kernel, tokens),
        jax.ShapeDtypeStruct((4 * tokens, 128), bf16),
        [ANY] * 4,
        [mixed] + [to_peer(mixed, 0, back) for back in range(1, 4)],
        scratch=[pltpu.SemaphoreType.DMA((4,))],
        flops=1_000_000,
        vmem=4,
    )
    mixes_other = shift(mixes, C, 1)
    rows_here = jax.ShapeDtypeStruct((512, 2048), bf16)
    middle, normed = call(
        middle_kernel,
        [rows_here] * 2,
        [VM] * 5,
        (early_own, early_other, norm_gain.reshape(1, -1), mixes, mixes_other),
        scratch=[
            pltpu.VMEM((512, 2048), bf16),
            pltpu.VMEM((512, 512), bf16),
            pltpu.VMEM((512, 2048), f32),
        ],
        flops=2 * 512 * 512 * 2048,
    )
    early_slots = tuple(range(7))
    summed = call(
        functools.partial(up_kernel, early_slots, False),
        jax.ShapeDtypeStruct((512, 1024), f32),
        [VM] * 8,
        (normed, *up_units[:7]),
        scratch=[pltpu.VMEM((2048, 1024), bf16)],
        flops=2 * 512 * 1024 * 1792,
    )
    hidden = call(
        functools.partial(up_kernel, (7,), True),
        jax.ShapeDtypeStruct((512, 1024), bf16),
        [VM] * 4,
        (normed, far_up, far_down, summed),
        scratch=[pltpu.VMEM((256, 1024), bf16)],
        flops=2 * 512 * 1024 * 256,
    )
    hidden_other = shift(hidden, C, 1)
    pieces = (down_columns, before, after, far_a, far_b)
    space = pltpu.VMEM((1024, 1024), bf16)
    partial = call(
        functools.partial(down_kernel, False),
        jax.ShapeDtypeStruct((512, 1024), f32),
        [VM] * 6,
        (hidden, *pieces),
        scratch=[space],
        flops=512 * 1024 * 2048,
    )
    sent = call(
        functools.partial(down_kernel, True),
        [jax.ShapeDtypeStruct((64, 1024), bf16)] * 8,
        [VM] * 7,
        (hidden_other, *pieces, partial),
        scratch=[space, pltpu.VMEM((512, 1024), bf16)],
        flops=512 * 1024 * 2048,
    )
    terms = [sent[0]] + [to_peer(sent[k], *peer) for k, peer in enumerate(peers) if k]
    return call(
        last_kernel,
        jax.ShapeDtypeStruct((64, 2048), bf16),
        [VM] * 9,
        (middle, *terms),
        scratch=[pltpu.VMEM((1024, 512), bf16)],
        flops=2 * 1024 * 512 * 512,
    )


def solution(mesh):
    torus = Mesh(mesh.devices.reshape(8, 4, 2, mesh.shape["tp"]), SP_TP)
    in_specs = (
        P(SP_TP, None),
        P(SP, "tp"),
        P(SP, "tp"),
        P(SP, "tp"),
        P("tp", SP),
        P("tp", SP),
        P(SP),
        P("tp", None),
        P(),
        P(SP, "tp"),
        P("tp", SP),
    )
    out_specs = P(SP_TP, None)
    return jax.shard_map(layer, mesh=torus, in_specs=in_specs, out_specs=out_specs, check_vma=False)
```

profile of v0, /device:TPU:2, one launch (start us, length us, event | category | flops | bytes accessed | tf_op | source)
XLA Modules:
  0.0 197.0 jit_solution(15818963487196113313)
XLA Ops:
  0.0 1.0 copy-done.1
  2.2 1.3 copy-done
  3.6 4.6 %all-to-all-start = ((bf16[4,128,2048]{2,1,0:T(8,128)(2,1)}), bf16[4,128,2048]{2,1,0:T(8,128)(2,1)S(1)}, u32[]{:S(2)}, u32[]{:S(2)}) async-start(bf16[4,128,2048]{2,1,0:T(8,128)(2,1)} %copy-done), calls=%async_computation | async-start | bytes 4194304 | tf_op jit(solution)/shard_map/all_to_all | solution.py:431
  8.4 26.2 %all-to-all-done.early_own = bf16[4,128,2048]{2,1,0:T(8,128)(2,1)S(1)} async-done(((bf16[4,128,2048]{2,1,0:T(8,128)(2,1)}), bf16[4,128,2048]{2,1,0:T(8,128)(2,1)S(1)}, u32[]{:S(2)}, u32[]{:S(2)}) %all-to-all-start) | async-done | bytes 2097184 | tf_op jit(solution)/shard_map/all_to_all | solution.py:431
  34.6 1.6 collective-permute-start.11
  36.7 2.1 %collective-permute-start.13 = (bf16[64,1024]{1,0:T(8,128)(2,1)S(1)}, bf16[64,1024]{1,0:T(8,128)(2,1)S(1)}, u32[]{:S(2)}, u32[]{:S(2)}) collective-permute-start(bf16[64,1024]{1,0:T(8,128)(2,1)S(1)} %maximum_select_fusion.refs_0_), channel_id=1, source_target_pairs={{0,16},{8,24},{16,0},{24,8},{1,17},{9,25},{17,1},{25,9},{2,18},{10... | collective-permute-start | bytes 393224 | tf_op jit(solution)/shard_map/ppermute | solution.py:305
  38.8 1.8 collective-permute-done.11.refs_1_
  40.6 1.3 collective-permute-done.12.refs_2_
  41.9 3.3 %collective-permute-done.13.refs_3_ = bf16[64,1024]{1,0:T(8,128)(2,1)S(1)} collective-permute-done((bf16[64,1024]{1,0:T(8,128)(2,1)S(1)}, bf16[64,1024]{1,0:T(8,128)(2,1)S(1)}, u32[]{:S(2)}, u32[]{:S(2)}) %collective-permute-start.13) | collective-permute-done | bytes 131104 | tf_op jit(solution)/shard_map/ppermute | solution.py:305
  45.9 2.0 %collective-permute-start.14 = (bf16[256,1024]{1,0:T(8,128)(2,1)S(1)}, bf16[256,1024]{1,0:T(8,128)(2,1)S(1)}, u32[]{:S(2)}, u32[]{:S(2)}) collective-permute-start(bf16[256,1024]{1,0:T(8,128)(2,1)S(1)} %shard_map.115.refs_0_), channel_id=1, source_target_pairs={{0,32},{32,64},{64,96},{96,128},{128,160},{160,192},{192,224},{224... | collective-permute-start | bytes 1572872 | tf_op jit(solution)/shard_map/ppermute | solution.py:305
  47.9 4.0 %collective-permute-start.17 = (bf16[256,1024]{1,0:T(8,128)(2,1)S(1)}, bf16[256,1024]{1,0:T(8,128)(2,1)S(1)}, u32[]{:S(2)}, u32[]{:S(2)}) collective-permute-start(bf16[256,1024]{1,0:T(8,128)(2,1)S(1)} %shard_map.115.refs_0_), channel_id=1, source_target_pairs={{0,224},{32,0},{64,32},{96,64},{128,96},{160,128},{192,160},{224,1... | collective-permute-start | bytes 1572872 | tf_op jit(solution)/shard_map/ppermute | solution.py:305
  52.0 11.4 %collective-permute-done.14.refs_1_ = bf16[256,1024]{1,0:T(8,128)(2,1)S(1)} collective-permute-done((bf16[256,1024]{1,0:T(8,128)(2,1)S(1)}, bf16[256,1024]{1,0:T(8,128)(2,1)S(1)}, u32[]{:S(2)}, u32[]{:S(2)}) %collective-permute-start.14) | collective-permute-done | bytes 524320 | tf_op jit(solution)/shard_map/ppermute | solution.py:305
  63.4 2.2 %shard_map.110 = (f32[72,128]{1,0:T(8,128)S(1)}, f32[256,768]{1,0:T(8,128)S(1)}) custom-call(f32[2,256]{1,0:T(2,128)S(1)} %copy-done.7, f32[2,256]{1,0:T(2,128)S(1)} %copy-done.8, s32[1,256]{1,0:T(1,128)S(1)} %bitcast.5, bf16[256,128]{1,0:T(8,128)(2,1)S(1)} %copy-done.4, bf16[256,128]{1,0:T(8,128)(2,1)S(1)} %copy-done.5, bf16[256,128]{1,0:T(8,128)(2,1)S(1)} %copy-done.6), custom_call_target="tpu_custom_call" | custom-call | flops 150000000 | bytes 1 | tf_op jit(solution)/shard_map/pallas_call | solution.py:30
  65.7 3.3 %collective-permute-start.18 = (bf16[256,1024]{1,0:T(8,128)(2,1)S(1)}, bf16[256,1024]{1,0:T(8,128)(2,1)S(1)}, u32[]{:S(2)}, u32[]{:S(2)}) collective-permute-start(bf16[256,1024]{1,0:T(8,128)(2,1)S(1)} %collective-permute-done.17.refs_2_), channel_id=1, source_target_pairs={{0,224},{32,0},{64,32},{96,64},{128,96},{160,128},{192,160},{224,1... | collective-permute-start | bytes 1572872 | tf_op jit(solution)/shard_map/ppermute | solution.py:305
  69.6 8.0 %collective-permute-start.2 = (f32[72,128]{1,0:T(8,128)S(1)}, f32[72,128]{1,0:T(8,128)S(1)}, u32[]{:S(2)}, u32[]{:S(2)}) collective-permute-start(f32[72,128]{1,0:T(8,128)S(1)} %get-tuple-element.22.refs_0_), channel_id=1, source_target_pairs={{0,16},{8,24},{16,32},{24,40},{32,48},{40,56},{48,64},{56,72},{64,... | collective-permute-start | bytes 110600 | tf_op jit(solution)/shard_map/ppermute | solution.py:409
  77.5 4.6 %collective-permute-done.2.refs_2_ = f32[72,128]{1,0:T(8,128)S(1)} collective-permute-done((f32[72,128]{1,0:T(8,128)S(1)}, f32[72,128]{1,0:T(8,128)S(1)}, u32[]{:S(2)}, u32[]{:S(2)}) %collective-permute-start.2) | collective-permute-done | bytes 36896 | tf_op jit(solution)/shard_map/ppermute | solution.py:409
  82.2 4.2 %collective-permute-start.3 = (f32[72,128]{1,0:T(8,128)S(1)}, f32[72,128]{1,0:T(8,128)S(1)}, u32[]{:S(2)}, u32[]{:S(2)}) collective-permute-start(f32[72,128]{1,0:T(8,128)S(1)} %get-tuple-element.22.refs_0_), channel_id=1, source_target_pairs={{0,24},{8,32},{16,40},{24,48},{32,56},{40,64},{48,72},{56,80},{64,... | collective-permute-start | bytes 110600 | tf_op jit(solution)/shard_map/ppermute | solution.py:409
  86.4 2.3 %collective-permute-done.3.refs_3_ = f32[72,128]{1,0:T(8,128)S(1)} collective-permute-done((f32[72,128]{1,0:T(8,128)S(1)}, f32[72,128]{1,0:T(8,128)S(1)}, u32[]{:S(2)}, u32[]{:S(2)}) %collective-permute-start.3) | collective-permute-done | bytes 36896 | tf_op jit(solution)/shard_map/ppermute | solution.py:409
  88.7 6.7 %collective-permute-done.4.refs_4_ = f32[72,128]{1,0:T(8,128)S(1)} collective-permute-done((f32[72,128]{1,0:T(8,128)S(1)}, f32[72,128]{1,0:T(8,128)S(1)}, u32[]{:S(2)}, u32[]{:S(2)}) %collective-permute-start.4) | collective-permute-done | bytes 36896 | tf_op jit(solution)/shard_map/ppermute | solution.py:409
  95.4 2.0 %collective-permute-start.24 = (bf16[32,2048]{1,0:T(8,128)(2,1)S(1)}, bf16[32,2048]{1,0:T(8,128)(2,1)S(1)}, u32[]{:S(2)}, u32[]{:S(2)}) collective-permute-start(bf16[32,2048]{1,0:T(8,128)(2,1)S(1)} %bitcast.3), channel_id=1, source_target_pairs={{0,224},{32,0},{64,32},{96,64},{128,96},{160,128},{192,160},{224,1... | collective-permute-start | bytes 393224 | tf_op jit(solution)/shard_map/ppermute | solution.py:305
  97.9 2.5 %collective-permute-done.24.refs_2_ = bf16[32,2048]{1,0:T(8,128)(2,1)S(1)} collective-permute-done((bf16[32,2048]{1,0:T(8,128)(2,1)S(1)}, bf16[32,2048]{1,0:T(8,128)(2,1)S(1)}, u32[]{:S(2)}, u32[]{:S(2)}) %collective-permute-start.24) | collective-permute-done | bytes 131104 | tf_op jit(solution)/shard_map/ppermute | solution.py:305
  100.5 3.1 %collective-permute-start.26 = (bf16[32,2048]{1,0:T(8,128)(2,1)S(1)}, bf16[32,2048]{1,0:T(8,128)(2,1)S(1)}, u32[]{:S(2)}, u32[]{:S(2)}) collective-permute-start(bf16[32,2048]{1,0:T(8,128)(2,1)S(1)} %collective-permute-done.24.refs_2_), channel_id=1, source_target_pairs={{0,224},{32,0},{64,32},{96,64},{128,96},{160,128},{192,160},{224,1... | collective-permute-start | bytes 393224 | tf_op jit(solution)/shard_map/ppermute | solution.py:305
  103.6 12.5 %collective-permute-done.25.refs_3_ = bf16[32,2048]{1,0:T(8,128)(2,1)S(1)} collective-permute-done((bf16[32,2048]{1,0:T(8,128)(2,1)S(1)}, bf16[32,2048]{1,0:T(8,128)(2,1)S(1)}, u32[]{:S(2)}, u32[]{:S(2)}) %collective-permute-start.25) | collective-permute-done | bytes 131104 | tf_op jit(solution)/shard_map/ppermute | solution.py:305
  117.2 3.2 %collective-permute-start.19 = (bf16[256,1024]{1,0:T(8,128)(2,1)S(1)}, bf16[256,1024]{1,0:T(8,128)(2,1)S(1)}, u32[]{:S(2)}, u32[]{:S(2)}) collective-permute-start(bf16[256,1024]{1,0:T(8,128)(2,1)S(1)} %collective-permute-done.18.refs_4_), channel_id=1, source_target_pairs={{0,224},{32,0},{64,32},{96,64},{128,96},{160,128},{192,160},{224,1... | collective-permute-start | bytes 1572872 | tf_op jit(solution)/shard_map/ppermute | solution.py:305
  120.4 1.7 collective-permute-done.6.refs_1_
  122.1 3.2 %collective-permute-start.28 = (bf16[32,2048]{1,0:T(8,128)(2,1)S(1)}, bf16[32,2048]{1,0:T(8,128)(2,1)S(1)}, u32[]{:S(2)}, u32[]{:S(2)}) collective-permute-start(bf16[32,2048]{1,0:T(8,128)(2,1)S(1)} %collective-permute-done.26.refs_4_), channel_id=1, source_target_pairs={{0,224},{32,0},{64,32},{96,64},{128,96},{160,128},{192,160},{224,1... | collective-permute-start | bytes 393224 | tf_op jit(solution)/shard_map/ppermute | solution.py:305
  125.4 8.2 %collective-permute-done.28.refs_6_ = bf16[32,2048]{1,0:T(8,128)(2,1)S(1)} collective-permute-done((bf16[32,2048]{1,0:T(8,128)(2,1)S(1)}, bf16[32,2048]{1,0:T(8,128)(2,1)S(1)}, u32[]{:S(2)}, u32[]{:S(2)}) %collective-permute-start.28) | collective-permute-done | bytes 131104 | tf_op jit(solution)/shard_map/ppermute | solution.py:305
  133.6 2.1 %collective-permute-start.7 = (bf16[256,128]{1,0:T(8,128)(2,1)S(1)}, bf16[256,128]{1,0:T(8,128)(2,1)S(1)}, u32[]{:S(2)}, u32[]{:S(2)}) collective-permute-start(bf16[256,128]{1,0:T(8,128)(2,1)S(1)} %shard_map.112.refs_0_), channel_id=1, source_target_pairs={{0,2},{1,3},{2,0},{3,1},{4,6},{5,7},{6,4},{7,5},{8,10},{9,11},{10,... | collective-permute-start | bytes 196616 | tf_op jit(solution)/shard_map/ppermute | solution.py:310
  135.7 1.0 collective-permute-start.8
  136.7 1.4 shard_map.119.mine
  138.1 1.3 collective-permute-done.7.refs_2_
  140.1 3.0 %collective-permute-start.31 = (bf16[256,2048]{1,0:T(8,128)(2,1)S(1)}, bf16[256,2048]{1,0:T(8,128)(2,1)S(1)}, u32[]{:S(2)}, u32[]{:S(2)}) collective-permute-start(bf16[256,2048]{1,0:T(8,128)(2,1)S(1)} %shard_map.119.mine), channel_id=1, source_target_pairs={{0,24},{8,0},{16,8},{24,16},{1,25},{9,1},{17,9},{25,17},{2,26},{10... | collective-permute-start | bytes 3145736 | tf_op jit(solution)/shard_map/ppermute | solution.py:305
  145.1 3.7 %collective-permute-start.21 = (bf16[128,1024]{1,0:T(8,128)(2,1)S(1)}, bf16[128,1024]{1,0:T(8,128)(2,1)S(1)}, u32[]{:S(2)}, u32[]{:S(2)}) collective-permute-start(bf16[128,1024]{1,0:T(8,128)(2,1)S(1)} %get-tuple-element.26), channel_id=1, source_target_pairs={{0,224},{32,0},{64,32},{96,64},{128,96},{160,128},{192,160},{224,1... | collective-permute-start | bytes 786440 | tf_op jit(solution)/shard_map/ppermute | solution.py:305
  148.7 3.4 %shard_map.114 = (bf16[512,2048]{1,0:T(8,128)(2,1)S(1)}, bf16[512,2048]{1,0:T(8,128)(2,1)S(1)}) custom-call(bf16[4,128,2048]{2,1,0:T(8,128)(2,1)S(1)} %all-to-all-done.early_own, bf16[4,128,2048]{2,1,0:T(8,128)(2,1)S(1)} %collective-permute-done.early_other, bf16[1,2048]{1,0:T(2,128)(2,1)S(1)} %reshape.6.gain, bf16[1024,128]{1,0:T(8,128)(2,1)S(1)} %shard_map.113.mixes_own, ...), custom_call_target="tpu_custom_call" | custom-call | flops 1073741824 | bytes 1 | tf_op jit(solution)/shard_map/pallas_call | solution.py:30
  152.2 3.2 %shard_map.117.refs_2_ = f32[512,1024]{1,0:T(8,128)S(1)} custom-call(bf16[512,2048]{1,0:T(8,128)(2,1)S(1)} %get-tuple-element.24.normed, bf16[256,1024]{1,0:T(8,128)(2,1)S(1)} %shard_map.115.refs_0_, bf16[256,1024]{1,0:T(8,128)(2,1)S(1)} %collective-permute-done.14.refs_1_, bf16[256,1024]{1,0:T(8,128)(2,1)S(1)} %collective-permute-done.17.refs_2_, ...), custom_call_target="tpu_custom_call" | custom-call | flops 1879048192 | bytes 1 | tf_op jit(solution)/shard_map/pallas_call | solution.py:30
  155.4 1.0 shard_map.118.hidden
  156.5 6.2 %collective-permute-done.30.one.before = bf16[256,2048]{1,0:T(8,128)(2,1)S(1)} collective-permute-done((bf16[256,2048]{1,0:T(8,128)(2,1)S(1)}, bf16[256,2048]{1,0:T(8,128)(2,1)S(1)}, u32[]{:S(2)}, u32[]{:S(2)}) %collective-permute-start.30) | collective-permute-done | bytes 1048608 | tf_op jit(solution)/shard_map/ppermute | solution.py:305
  163.3 2.0 %collective-permute-start.32 = (bf16[128,2048]{1,0:T(8,128)(2,1)S(1)}, bf16[128,2048]{1,0:T(8,128)(2,1)S(1)}, u32[]{:S(2)}, u32[]{:S(2)}) collective-permute-start(bf16[128,2048]{1,0:T(8,128)(2,1)S(1)} %get-tuple-element.27), channel_id=1, source_target_pairs={{0,8},{8,16},{16,24},{24,0},{1,9},{9,17},{17,25},{25,1},{2,10},{10... | collective-permute-start | bytes 1572872 | tf_op jit(solution)/shard_map/ppermute | solution.py:305
  165.9 8.1 %collective-permute-done.32.far_a = bf16[128,2048]{1,0:T(8,128)(2,1)S(1)} collective-permute-done((bf16[128,2048]{1,0:T(8,128)(2,1)S(1)}, bf16[128,2048]{1,0:T(8,128)(2,1)S(1)}, u32[]{:S(2)}, u32[]{:S(2)}) %collective-permute-start.32) | collective-permute-done | bytes 524320 | tf_op jit(solution)/shard_map/ppermute | solution.py:305
  174.1 1.8 collective-permute-done.33.far_b
  175.9 2.0 %shard_map.121.refs_0_ = f32[512,1024]{1,0:T(8,128)S(1)} custom-call(bf16[512,1024]{1,0:T(8,128)(2,1)S(1)} %shard_map.118.hidden, bf16[256,2048]{1,0:T(8,128)(2,1)S(1)} %shard_map.119.mine, bf16[256,2048]{1,0:T(8,128)(2,1)S(1)} %collective-permute-done.30.one.before, bf16[256,2048]{1,0:T(8,128)(2,1)S(1)} %collective-permute-done.31.two.after, ...), custom_call_target="tpu_custom_call" | custom-call | flops 1073741824 | bytes 1 | tf_op jit(solution)/shard_map/pallas_call | solution.py:30
  177.9 2.2 %shard_map.122 = (bf16[64,1024]{1,0:T(8,128)(2,1)S(1)}, bf16[64,1024]{1,0:T(8,128)(2,1)S(1)}, bf16[64,1024]{1,0:T(8,128)(2,1)S(1)}, bf16[64,1024]{1,0:T(8,128)(2...) custom-call(bf16[512,1024]{1,0:T(8,128)(2,1)S(1)} %collective-permut, ...), custom_call_target="tpu_custom_call" | custom-call | flops 1073741824 | bytes 1 | tf_op jit(solution)/shard_map/pallas_call | solution.py:30
  180.1 1.0 collective-permute-start.34
  181.1 3.3 %collective-permute-start.35 = (bf16[64,1024]{1,0:T(8,128)(2,1)S(1)}, bf16[64,1024]{1,0:T(8,128)(2,1)S(1)}, u32[]{:S(2)}, u32[]{:S(2)}) collective-permute-start(bf16[64,1024]{1,0:T(8,128)(2,1)S(1)} %get-tuple-element.31), channel_id=1, source_target_pairs={{0,2},{1,3},{2,0},{3,1},{4,6},{5,7},{6,4},{7,5},{8,10},{9,11},{10,... | collective-permute-start | bytes 393224 | tf_op jit(solution)/shard_map/ppermute | solution.py:310
  184.9 1.6 collective-permute-start.38
  186.5 3.2 %collective-permute-done.35.refs_2_ = bf16[64,1024]{1,0:T(8,128)(2,1)S(1)} collective-permute-done((bf16[64,1024]{1,0:T(8,128)(2,1)S(1)}, bf16[64,1024]{1,0:T(8,128)(2,1)S(1)}, u32[]{:S(2)}, u32[]{:S(2)}) %collective-permute-start.35) | collective-permute-done | bytes 131104 | tf_op jit(solution)/shard_map/ppermute | solution.py:310
  189.7 4.9 %collective-permute-done.38.refs_5_ = bf16[64,1024]{1,0:T(8,128)(2,1)S(1)} collective-permute-done((bf16[64,1024]{1,0:T(8,128)(2,1)S(1)}, bf16[64,1024]{1,0:T(8,128)(2,1)S(1)}, u32[]{:S(2)}, u32[]{:S(2)}) %collective-permute-start.38) | collective-permute-done | bytes 131104 | tf_op jit(solution)/shard_map/ppermute | solution.py:310
  195.5 1.5 shard_map.123
  (78 shorter events, 10.3 us)
Async XLA Ops:
  3.6 59.8 %copy-start.6 = (bf16[256,128]{1,0:T(8,128)(2,1)S(1)}, bf16[256,128]{1,0:T(8,128)(2,1)}, u32[]{:S(2)}) copy-start(bf16[256,128]{1,0:T(8,128)(2,1)} %refs_5_.1) | copy-start | bytes 196612
  3.6 59.8 %copy-start.7 = (f32[2,256]{1,0:T(2,128)S(1)}, f32[2,256]{1,0:T(2,128)}, u32[]{:S(2)}) copy-start(f32[2,256]{1,0:T(2,128)} %refs_0_.1) | copy-start | bytes 6148
  3.6 59.8 %copy-start.8 = (f32[2,256]{1,0:T(2,128)S(1)}, f32[2,256]{1,0:T(2,128)}, u32[]{:S(2)}) copy-start(f32[2,256]{1,0:T(2,128)} %refs_1_.1) | copy-start | bytes 6148
  3.6 59.8 %copy-start.9 = (s32[256]{0:T(256)S(1)}, s32[256]{0:T(256)}, u32[]{:S(2)}) copy-start(s32[256]{0:T(256)} %param.17) | copy-start | bytes 3076
  3.6 30.9 %all-to-all-start = ((bf16[4,128,2048]{2,1,0:T(8,128)(2,1)}), bf16[4,128,2048]{2,1,0:T(8,128)(2,1)S(1)}, u32[]{:S(2)}, u32[]{:S(2)}) async-start(bf16[4,128,2048]{2,1,0:T(8,128)(2,1)} %copy-done), calls=%async_computation | async-start | bytes 4194304 | tf_op jit(solution)/shard_map/all_to_all | solution.py:431
  8.2 60.7 %copy-start.3 = (bf16[2048,32]{0,1:T(8,128)(2,1)S(1)}, bf16[2048,32]{0,1:T(8,128)(2,1)}, u32[]{:S(2)}) copy-start(bf16[2048,32]{0,1:T(8,128)(2,1)} %param.21) | copy-start | bytes 393220
  8.3 26.3 %collective-permute-start.10 = (bf16[32,1024]{1,0:T(8,128)(2,1)S(1)}, bf16[32,1024]{1,0:T(8,128)(2,1)S(1)}, u32[]{:S(2)}, u32[]{:S(2)}) collective-permute-start(bf16[32,1024]{1,0:T(8,128)(2,1)S(1)} %get-tuple-element.38), channel_id=1, source_target_pairs={{0,4},{4,0},{1,5},{5,1},{2,6},{6,2},{3,7},{7,3},{8,12},{12,8},{9,1... | collective-permute-start | bytes 196616 | tf_op jit(solution)/shard_map/ppermute | solution.py:305
  34.6 114.2 %collective-permute-start = (bf16[4,128,2048]{2,1,0:T(8,128)(2,1)S(1)}, bf16[4,128,2048]{2,1,0:T(8,128)(2,1)S(1)}, u32[]{:S(2)}, u32[]{:S(2)}) collective-permute-start(bf16[4,128,2048]{2,1,0:T(8,128)(2,1)S(1)} %all-to-all-done.early_own), channel_id=1, source_target_pairs={{0,4},{4,0},{1,5},{5,1},{2,6},{6,2},{3,7},{7,3},{8,12},{12,8},{9,1... | collective-permute-start | bytes 6291464 | tf_op jit(solution)/shard_map/ppermute | solution.py:305
  34.6 6.0 %collective-permute-start.11 = (bf16[64,1024]{1,0:T(8,128)(2,1)S(1)}, bf16[64,1024]{1,0:T(8,128)(2,1)S(1)}, u32[]{:S(2)}, u32[]{:S(2)}) collective-permute-start(bf16[64,1024]{1,0:T(8,128)(2,1)S(1)} %maximum_select_fusion.refs_0_), channel_id=1, source_target_pairs={{0,8},{8,16},{16,24},{24,0},{1,9},{9,17},{17,25},{25,1},{2,10},{10... | collective-permute-start | bytes 393224 | tf_op jit(solution)/shard_map/ppermute | solution.py:305
  36.2 5.7 %collective-permute-start.12 = (bf16[64,1024]{1,0:T(8,128)(2,1)S(1)}, bf16[64,1024]{1,0:T(8,128)(2,1)S(1)}, u32[]{:S(2)}, u32[]{:S(2)}) collective-permute-start(bf16[64,1024]{1,0:T(8,128)(2,1)S(1)} %maximum_select_fusion.refs_0_), channel_id=1, source_target_pairs={{0,24},{8,0},{16,8},{24,16},{1,25},{9,1},{17,9},{25,17},{2,26},{10... | collective-permute-start | bytes 393224 | tf_op jit(solution)/shard_map/ppermute | solution.py:305
  36.7 8.5 %collective-permute-start.13 = (bf16[64,1024]{1,0:T(8,128)(2,1)S(1)}, bf16[64,1024]{1,0:T(8,128)(2,1)S(1)}, u32[]{:S(2)}, u32[]{:S(2)}) collective-permute-start(bf16[64,1024]{1,0:T(8,128)(2,1)S(1)} %maximum_select_fusion.refs_0_), channel_id=1, source_target_pairs={{0,16},{8,24},{16,0},{24,8},{1,17},{9,25},{17,1},{25,9},{2,18},{10... | collective-permute-start | bytes 393224 | tf_op jit(solution)/shard_map/ppermute | solution.py:305
  45.9 17.4 %collective-permute-start.14 = (bf16[256,1024]{1,0:T(8,128)(2,1)S(1)}, bf16[256,1024]{1,0:T(8,128)(2,1)S(1)}, u32[]{:S(2)}, u32[]{:S(2)}) collective-permute-start(bf16[256,1024]{1,0:T(8,128)(2,1)S(1)} %shard_map.115.refs_0_), channel_id=1, source_target_pairs={{0,32},{32,64},{64,96},{96,128},{128,160},{160,192},{192,224},{224... | collective-permute-start | bytes 1572872 | tf_op jit(solution)/shard_map/ppermute | solution.py:305
  47.9 17.7 %collective-permute-start.17 = (bf16[256,1024]{1,0:T(8,128)(2,1)S(1)}, bf16[256,1024]{1,0:T(8,128)(2,1)S(1)}, u32[]{:S(2)}, u32[]{:S(2)}) collective-permute-start(bf16[256,1024]{1,0:T(8,128)(2,1)S(1)} %shard_map.115.refs_0_), channel_id=1, source_target_pairs={{0,224},{32,0},{64,32},{96,64},{128,96},{160,128},{192,160},{224,1... | collective-permute-start | bytes 1572872 | tf_op jit(solution)/shard_map/ppermute | solution.py:305
  63.3 34.4 %collective-permute-start.15 = (bf16[256,1024]{1,0:T(8,128)(2,1)S(1)}, bf16[256,1024]{1,0:T(8,128)(2,1)S(1)}, u32[]{:S(2)}, u32[]{:S(2)}) collective-permute-start(bf16[256,1024]{1,0:T(8,128)(2,1)S(1)} %collective-permute-done.14.refs_1_), channel_id=1, source_target_pairs={{0,32},{32,64},{64,96},{96,128},{128,160},{160,192},{192,224},{224... | collective-permute-start | bytes 1572872 | tf_op jit(solution)/shard_map/ppermute | solution.py:305
  65.6 4.0 %collective-permute-start.1 = (f32[72,128]{1,0:T(8,128)S(1)}, f32[72,128]{1,0:T(8,128)S(1)}, u32[]{:S(2)}, u32[]{:S(2)}) collective-permute-start(f32[72,128]{1,0:T(8,128)S(1)} %get-tuple-element.22.refs_0_), channel_id=1, source_target_pairs={{0,8},{8,16},{16,24},{24,32},{32,40},{40,48},{48,56},{56,64},{64,7... | collective-permute-start | bytes 110600 | tf_op jit(solution)/shard_map/ppermute | solution.py:409
  65.7 51.6 %collective-permute-start.18 = (bf16[256,1024]{1,0:T(8,128)(2,1)S(1)}, bf16[256,1024]{1,0:T(8,128)(2,1)S(1)}, u32[]{:S(2)}, u32[]{:S(2)}) collective-permute-start(bf16[256,1024]{1,0:T(8,128)(2,1)S(1)} %collective-permute-done.17.refs_2_), channel_id=1, source_target_pairs={{0,224},{32,0},{64,32},{96,64},{128,96},{160,128},{192,160},{224,1... | collective-permute-start | bytes 1572872 | tf_op jit(solution)/shard_map/ppermute | solution.py:305
  69.0 74.6 %copy-start.11 = (bf16[2048]{0:T(1024)(128)(2,1)S(1)}, bf16[2048]{0:T(1024)(128)(2,1)}, u32[]{:S(2)}) copy-start(bf16[2048]{0:T(1024)(128)(2,1)} %param.19) | copy-start | bytes 12292
  69.0 28.7 %collective-permute-start.23 = (bf16[32,2048]{1,0:T(8,128)(2,1)S(1)}, bf16[32,2048]{1,0:T(8,128)(2,1)S(1)}, u32[]{:S(2)}, u32[]{:S(2)}) collective-permute-start(bf16[32,2048]{1,0:T(8,128)(2,1)S(1)} %bitcast.2), channel_id=1, source_target_pairs={{0,32},{32,64},{64,96},{96,128},{128,160},{160,192},{192,224},{224... | collective-permute-start | bytes 393224 | tf_op jit(solution)/shard_map/ppermute | solution.py:305
  69.6 12.6 %collective-permute-start.2 = (f32[72,128]{1,0:T(8,128)S(1)}, f32[72,128]{1,0:T(8,128)S(1)}, u32[]{:S(2)}, u32[]{:S(2)}) collective-permute-start(f32[72,128]{1,0:T(8,128)S(1)} %get-tuple-element.22.refs_0_), channel_id=1, source_target_pairs={{0,16},{8,24},{16,32},{24,40},{32,48},{40,56},{48,64},{56,72},{64,... | collective-permute-start | bytes 110600 | tf_op jit(solution)/shard_map/ppermute | solution.py:409
  82.2 6.5 %collective-permute-start.3 = (f32[72,128]{1,0:T(8,128)S(1)}, f32[72,128]{1,0:T(8,128)S(1)}, u32[]{:S(2)}, u32[]{:S(2)}) collective-permute-start(f32[72,128]{1,0:T(8,128)S(1)} %get-tuple-element.22.refs_0_), channel_id=1, source_target_pairs={{0,24},{8,32},{16,40},{24,48},{32,56},{40,64},{48,72},{56,80},{64,... | collective-permute-start | bytes 110600 | tf_op jit(solution)/shard_map/ppermute | solution.py:409
  88.7 6.7 %collective-permute-start.4 = (f32[72,128]{1,0:T(8,128)S(1)}, f32[72,128]{1,0:T(8,128)S(1)}, u32[]{:S(2)}, u32[]{:S(2)}) collective-permute-start(f32[72,128]{1,0:T(8,128)S(1)} %get-tuple-element.22.refs_0_), channel_id=1, source_target_pairs={{0,32},{8,40},{16,48},{24,56},{32,64},{40,72},{48,80},{56,88},{64,... | collective-permute-start | bytes 110600 | tf_op jit(solution)/shard_map/ppermute | solution.py:409
  95.4 5.0 %collective-permute-start.24 = (bf16[32,2048]{1,0:T(8,128)(2,1)S(1)}, bf16[32,2048]{1,0:T(8,128)(2,1)S(1)}, u32[]{:S(2)}, u32[]{:S(2)}) collective-permute-start(bf16[32,2048]{1,0:T(8,128)(2,1)S(1)} %bitcast.3), channel_id=1, source_target_pairs={{0,224},{32,0},{64,32},{96,64},{128,96},{160,128},{192,160},{224,1... | collective-permute-start | bytes 393224 | tf_op jit(solution)/shard_map/ppermute | solution.py:305
  97.7 2.8 %collective-permute-start.5 = (f32[360,128]{1,0:T(8,128)S(1)}, f32[360,128]{1,0:T(8,128)S(1)}, u32[]{:S(2)}, u32[]{:S(2)}) collective-permute-start(f32[360,128]{1,0:T(8,128)S(1)} %shard_map.111.states_own), channel_id=1, source_target_pairs={{0,4},{4,0},{1,5},{5,1},{2,6},{6,2},{3,7},{7,3},{8,12},{12,8},{9,1... | collective-permute-start | bytes 552968 | tf_op jit(solution)/shard_map/ppermute | solution.py:305
  97.8 45.7 %collective-permute-start.16 = (bf16[256,1024]{1,0:T(8,128)(2,1)S(1)}, bf16[256,1024]{1,0:T(8,128)(2,1)S(1)}, u32[]{:S(2)}, u32[]{:S(2)}) collective-permute-start(bf16[256,1024]{1,0:T(8,128)(2,1)S(1)} %collective-permute-done.15.refs_3_), channel_id=1, source_target_pairs={{0,32},{32,64},{64,96},{96,128},{128,160},{160,192},{192,224},{224... | collective-permute-start | bytes 1572872 | tf_op jit(solution)/shard_map/ppermute | solution.py:305
  100.3 15.8 %collective-permute-start.25 = (bf16[32,2048]{1,0:T(8,128)(2,1)S(1)}, bf16[32,2048]{1,0:T(8,128)(2,1)S(1)}, u32[]{:S(2)}, u32[]{:S(2)}) collective-permute-start(bf16[32,2048]{1,0:T(8,128)(2,1)S(1)} %collective-permute-done.23.refs_1_), channel_id=1, source_target_pairs={{0,32},{32,64},{64,96},{96,128},{128,160},{160,192},{192,224},{224... | collective-permute-start | bytes 393224 | tf_op jit(solution)/shard_map/ppermute | solution.py:305
  100.5 16.1 %collective-permute-start.26 = (bf16[32,2048]{1,0:T(8,128)(2,1)S(1)}, bf16[32,2048]{1,0:T(8,128)(2,1)S(1)}, u32[]{:S(2)}, u32[]{:S(2)}) collective-permute-start(bf16[32,2048]{1,0:T(8,128)(2,1)S(1)} %collective-permute-done.24.refs_2_), channel_id=1, source_target_pairs={{0,224},{32,0},{64,32},{96,64},{128,96},{160,128},{192,160},{224,1... | collective-permute-start | bytes 393224 | tf_op jit(solution)/shard_map/ppermute | solution.py:305
  116.1 9.2 %collective-permute-start.27 = (bf16[32,2048]{1,0:T(8,128)(2,1)S(1)}, bf16[32,2048]{1,0:T(8,128)(2,1)S(1)}, u32[]{:S(2)}, u32[]{:S(2)}) collective-permute-start(bf16[32,2048]{1,0:T(8,128)(2,1)S(1)} %collective-permute-done.25.refs_3_), channel_id=1, source_target_pairs={{0,32},{32,64},{64,96},{96,128},{128,160},{160,192},{192,224},{224... | collective-permute-start | bytes 393224 | tf_op jit(solution)/shard_map/ppermute | solution.py:305
  116.6 5.6 %collective-permute-start.6 = (bf16[256,128]{1,0:T(8,128)(2,1)S(1)}, bf16[256,128]{1,0:T(8,128)(2,1)S(1)}, u32[]{:S(2)}, u32[]{:S(2)}) collective-permute-start(bf16[256,128]{1,0:T(8,128)(2,1)S(1)} %shard_map.112.refs_0_), channel_id=1, source_target_pairs={{0,1},{1,2},{2,3},{3,0},{4,5},{5,6},{6,7},{7,4},{8,9},{9,10},{10,1... | collective-permute-start | bytes 196616 | tf_op jit(solution)/shard_map/ppermute | solution.py:310
  117.2 26.4 %collective-permute-start.19 = (bf16[256,1024]{1,0:T(8,128)(2,1)S(1)}, bf16[256,1024]{1,0:T(8,128)(2,1)S(1)}, u32[]{:S(2)}, u32[]{:S(2)}) collective-permute-start(bf16[256,1024]{1,0:T(8,128)(2,1)S(1)} %collective-permute-done.18.refs_4_), channel_id=1, source_target_pairs={{0,224},{32,0},{64,32},{96,64},{128,96},{160,128},{192,160},{224,1... | collective-permute-start | bytes 1572872 | tf_op jit(solution)/shard_map/ppermute | solution.py:305
  122.1 11.5 %collective-permute-start.28 = (bf16[32,2048]{1,0:T(8,128)(2,1)S(1)}, bf16[32,2048]{1,0:T(8,128)(2,1)S(1)}, u32[]{:S(2)}, u32[]{:S(2)}) collective-permute-start(bf16[32,2048]{1,0:T(8,128)(2,1)S(1)} %collective-permute-done.26.refs_4_), channel_id=1, source_target_pairs={{0,224},{32,0},{64,32},{96,64},{128,96},{160,128},{192,160},{224,1... | collective-permute-start | bytes 393224 | tf_op jit(solution)/shard_map/ppermute | solution.py:305
  125.4 10.3 %collective-permute-start.29 = (bf16[32,2048]{1,0:T(8,128)(2,1)S(1)}, bf16[32,2048]{1,0:T(8,128)(2,1)S(1)}, u32[]{:S(2)}, u32[]{:S(2)}) collective-permute-start(bf16[32,2048]{1,0:T(8,128)(2,1)S(1)} %collective-permute-done.27.refs_5_), channel_id=1, source_target_pairs={{0,32},{32,64},{64,96},{96,128},{128,160},{160,192},{192,224},{224... | collective-permute-start | bytes 393224 | tf_op jit(solution)/shard_map/ppermute | solution.py:305
  133.6 5.8 %collective-permute-start.7 = (bf16[256,128]{1,0:T(8,128)(2,1)S(1)}, bf16[256,128]{1,0:T(8,128)(2,1)S(1)}, u32[]{:S(2)}, u32[]{:S(2)}) collective-permute-start(bf16[256,128]{1,0:T(8,128)(2,1)S(1)} %shard_map.112.refs_0_), channel_id=1, source_target_pairs={{0,2},{1,3},{2,0},{3,1},{4,6},{5,7},{6,4},{7,5},{8,10},{9,11},{10,... | collective-permute-start | bytes 196616 | tf_op jit(solution)/shard_map/ppermute | solution.py:310
  135.7 4.4 %collective-permute-start.8 = (bf16[256,128]{1,0:T(8,128)(2,1)S(1)}, bf16[256,128]{1,0:T(8,128)(2,1)S(1)}, u32[]{:S(2)}, u32[]{:S(2)}) collective-permute-start(bf16[256,128]{1,0:T(8,128)(2,1)S(1)} %shard_map.112.refs_0_), channel_id=1, source_target_pairs={{0,3},{1,0},{2,1},{3,2},{4,7},{5,4},{6,5},{7,6},{8,11},{9,8},{10,9... | collective-permute-start | bytes 196616 | tf_op jit(solution)/shard_map/ppermute | solution.py:310
  139.4 23.3 %collective-permute-start.30 = (bf16[256,2048]{1,0:T(8,128)(2,1)S(1)}, bf16[256,2048]{1,0:T(8,128)(2,1)S(1)}, u32[]{:S(2)}, u32[]{:S(2)}) collective-permute-start(bf16[256,2048]{1,0:T(8,128)(2,1)S(1)} %shard_map.119.mine), channel_id=1, source_target_pairs={{0,8},{8,16},{16,24},{24,0},{1,9},{9,17},{17,25},{25,1},{2,10},{10... | collective-permute-start | bytes 3145736 | tf_op jit(solution)/shard_map/ppermute | solution.py:305
  140.1 23.1 %collective-permute-start.31 = (bf16[256,2048]{1,0:T(8,128)(2,1)S(1)}, bf16[256,2048]{1,0:T(8,128)(2,1)S(1)}, u32[]{:S(2)}, u32[]{:S(2)}) collective-permute-start(bf16[256,2048]{1,0:T(8,128)(2,1)S(1)} %shard_map.119.mine), channel_id=1, source_target_pairs={{0,24},{8,0},{16,8},{24,16},{1,25},{9,1},{17,9},{25,17},{2,26},{10... | collective-permute-start | bytes 3145736 | tf_op jit(solution)/shard_map/ppermute | solution.py:305
  143.5 1.6 collective-permute-start.9
  143.7 11.7 %collective-permute-start.20 = (bf16[128,1024]{1,0:T(8,128)(2,1)S(1)}, bf16[128,1024]{1,0:T(8,128)(2,1)S(1)}, u32[]{:S(2)}, u32[]{:S(2)}) collective-permute-start(bf16[128,1024]{1,0:T(8,128)(2,1)S(1)} %get-tuple-element.25), channel_id=1, source_target_pairs={{0,32},{32,64},{64,96},{96,128},{128,160},{160,192},{192,224},{224... | collective-permute-start | bytes 786440 | tf_op jit(solution)/shard_map/ppermute | solution.py:305
  145.1 10.3 %collective-permute-start.21 = (bf16[128,1024]{1,0:T(8,128)(2,1)S(1)}, bf16[128,1024]{1,0:T(8,128)(2,1)S(1)}, u32[]{:S(2)}, u32[]{:S(2)}) collective-permute-start(bf16[128,1024]{1,0:T(8,128)(2,1)S(1)} %get-tuple-element.26), channel_id=1, source_target_pairs={{0,224},{32,0},{64,32},{96,64},{128,96},{160,128},{192,160},{224,1... | collective-permute-start | bytes 786440 | tf_op jit(solution)/shard_map/ppermute | solution.py:305
  156.4 21.5 %collective-permute-start.22 = (bf16[512,1024]{1,0:T(8,128)(2,1)S(1)}, bf16[512,1024]{1,0:T(8,128)(2,1)S(1)}, u32[]{:S(2)}, u32[]{:S(2)}) collective-permute-start(bf16[512,1024]{1,0:T(8,128)(2,1)S(1)} %shard_map.118.hidden), channel_id=1, source_target_pairs={{0,4},{4,0},{1,5},{5,1},{2,6},{6,2},{3,7},{7,3},{8,12},{12,8},{9,1... | collective-permute-start | bytes 3145736 | tf_op jit(solution)/shard_map/ppermute | solution.py:305
  163.3 10.8 %collective-permute-start.32 = (bf16[128,2048]{1,0:T(8,128)(2,1)S(1)}, bf16[128,2048]{1,0:T(8,128)(2,1)S(1)}, u32[]{:S(2)}, u32[]{:S(2)}) collective-permute-start(bf16[128,2048]{1,0:T(8,128)(2,1)S(1)} %get-tuple-element.27), channel_id=1, source_target_pairs={{0,8},{8,16},{16,24},{24,0},{1,9},{9,17},{17,25},{25,1},{2,10},{10... | collective-permute-start | bytes 1572872 | tf_op jit(solution)/shard_map/ppermute | solution.py:305
  165.2 10.6 %collective-permute-start.33 = (bf16[128,2048]{1,0:T(8,128)(2,1)S(1)}, bf16[128,2048]{1,0:T(8,128)(2,1)S(1)}, u32[]{:S(2)}, u32[]{:S(2)}) collective-permute-start(bf16[128,2048]{1,0:T(8,128)(2,1)S(1)} %get-tuple-element.28), channel_id=1, source_target_pairs={{0,24},{8,0},{16,8},{24,16},{1,25},{9,1},{17,9},{25,17},{2,26},{10... | collective-permute-start | bytes 1572872 | tf_op jit(solution)/shard_map/ppermute | solution.py:305
  180.1 6.4 %collective-permute-start.34 = (bf16[64,1024]{1,0:T(8,128)(2,1)S(1)}, bf16[64,1024]{1,0:T(8,128)(2,1)S(1)}, u32[]{:S(2)}, u32[]{:S(2)}) collective-permute-start(bf16[64,1024]{1,0:T(8,128)(2,1)S(1)} %get-tuple-element.30), channel_id=1, source_target_pairs={{0,1},{1,2},{2,3},{3,0},{4,5},{5,6},{6,7},{7,4},{8,9},{9,10},{10,1... | collective-permute-start | bytes 393224 | tf_op jit(solution)/shard_map/ppermute | solution.py:310
  181.1 8.7 %collective-permute-start.35 = (bf16[64,1024]{1,0:T(8,128)(2,1)S(1)}, bf16[64,1024]{1,0:T(8,128)(2,1)S(1)}, u32[]{:S(2)}, u32[]{:S(2)}) collective-permute-start(bf16[64,1024]{1,0:T(8,128)(2,1)S(1)} %get-tuple-element.31), channel_id=1, source_target_pairs={{0,2},{1,3},{2,0},{3,1},{4,6},{5,7},{6,4},{7,5},{8,10},{9,11},{10,... | collective-permute-start | bytes 393224 | tf_op jit(solution)/shard_map/ppermute | solution.py:310
  184.4 5.4 %collective-permute-start.36 = (bf16[64,1024]{1,0:T(8,128)(2,1)S(1)}, bf16[64,1024]{1,0:T(8,128)(2,1)S(1)}, u32[]{:S(2)}, u32[]{:S(2)}) collective-permute-start(bf16[64,1024]{1,0:T(8,128)(2,1)S(1)} %get-tuple-element.32), channel_id=1, source_target_pairs={{0,3},{1,0},{2,1},{3,2},{4,7},{5,4},{6,5},{7,6},{8,11},{9,8},{10,9... | collective-permute-start | bytes 393224 | tf_op jit(solution)/shard_map/ppermute | solution.py:310
  184.9 4.9 %collective-permute-start.37 = (bf16[64,1024]{1,0:T(8,128)(2,1)S(1)}, bf16[64,1024]{1,0:T(8,128)(2,1)S(1)}, u32[]{:S(2)}, u32[]{:S(2)}) collective-permute-start(bf16[64,1024]{1,0:T(8,128)(2,1)S(1)} %get-tuple-element.33), channel_id=1, source_target_pairs={{0,4},{1,5},{2,6},{3,7},{4,0},{5,1},{6,2},{7,3},{8,12},{9,13},{10,... | collective-permute-start | bytes 393224 | tf_op jit(solution)/shard_map/ppermute | solution.py:310
  184.9 9.8 %collective-permute-start.38 = (bf16[64,1024]{1,0:T(8,128)(2,1)S(1)}, bf16[64,1024]{1,0:T(8,128)(2,1)S(1)}, u32[]{:S(2)}, u32[]{:S(2)}) collective-permute-start(bf16[64,1024]{1,0:T(8,128)(2,1)S(1)} %get-tuple-element.34), channel_id=1, source_target_pairs={{0,5},{1,6},{2,7},{3,4},{4,1},{5,2},{6,3},{7,0},{8,13},{9,14},{10,... | collective-permute-start | bytes 393224 | tf_op jit(solution)/shard_map/ppermute | solution.py:310
  186.5 8.2 %collective-permute-start.39 = (bf16[64,1024]{1,0:T(8,128)(2,1)S(1)}, bf16[64,1024]{1,0:T(8,128)(2,1)S(1)}, u32[]{:S(2)}, u32[]{:S(2)}) collective-permute-start(bf16[64,1024]{1,0:T(8,128)(2,1)S(1)} %get-tuple-element.35), channel_id=1, source_target_pairs={{0,6},{1,7},{2,4},{3,5},{4,2},{5,3},{6,0},{7,1},{8,14},{9,15},{10,... | collective-permute-start | bytes 393224 | tf_op jit(solution)/shard_map/ppermute | solution.py:310
  189.7 5.8 %collective-permute-start.40 = (bf16[64,1024]{1,0:T(8,128)(2,1)S(1)}, bf16[64,1024]{1,0:T(8,128)(2,1)S(1)}, u32[]{:S(2)}, u32[]{:S(2)}) collective-permute-start(bf16[64,1024]{1,0:T(8,128)(2,1)S(1)} %get-tuple-element.36), channel_id=1, source_target_pairs={{0,7},{1,4},{2,5},{3,6},{4,3},{5,0},{6,1},{7,2},{8,15},{9,12},{10,... | collective-permute-start | bytes 393224 | tf_op jit(solution)/shard_map/ppermute | solution.py:310
  (6 other events, 127.5 us)
where the time goes:
time: 199 us; the launch traced here: 197 us
  waiting for transfers between devices  112 us (56%)
  starting transfers between devices  62.7 us (32%)
  Pallas kernels  19 us (10%)
  local copies, waits for them, and re-layouts  3.38 us (2%)
    ppermute x27, waiting for transfers between devices, shift(): return lax.ppermute(value, axis, [(i, (i + by) % n) for i in range(n)])  58.4 us
    ppermute x27, starting transfers between devices, shift(): return lax.ppermute(value, axis, [(i, (i + by) % n) for i in range(n)])  35.7 us
    all_to_all x1, waiting for transfers between devices, layer(): early_own = lax.all_to_all(early, Y, 0, 0, tiled=True)  26.2 us
    pallas_call x15, Pallas kernels, call(): pl.pallas_call(kernel, out_shape=outs, in_specs=ins, out_specs=[VM] * len...  19 us
    ppermute x4, waiting for transfers between devices, layer(): lax.ppermute(state, (Z, X), [(i, (i + back) % 32) for i in range(32)])  14.2 us
    ppermute x10, waiting for transfers between devices, to_peer(): return lax.ppermute(value, (C, Y), pairs)  12.7 us
    ppermute x4, starting transfers between devices, layer(): lax.ppermute(state, (Z, X), [(i, (i + back) % 32) for i in range(32)])  12.3 us
    ppermute x10, starting transfers between devices, to_peer(): return lax.ppermute(value, (C, Y), pairs)  10.1 us
  transfers between devices with their start and end apart: 42, of which 23 were waited for; matrix products, arithmetic and copies ran while one was open for 0% of the time, Pallas kernels for 8%

commit v1 on v0

--- a/solution.py
+++ b/solution.py
@@ -210,32 +210,27 @@
 X_OFFSETS = (0, -1, 1, 2)
 
 
-def up_kernel(slots, final, normed, *refs):
-    if final:
-        units, (before, out, weights) = refs[:2], refs[2:]
-    else:
-        units, (out, weights) = refs[:len(slots)], refs[len(slots):]
+def up_kernel(slots, first, final, normed, *refs):
+    count = len(slots) + final
+    units, refs = refs[:count], refs[count:]
+    before, (out, weights, left) = (None, refs) if first else (refs[0], refs[1:])
     z, x = lax.axis_index(Z), lax.axis_index(X)
     for j, slot in enumerate(slots):
-        chunk = 0 if final else (z + 8 + OFFSETS[slot]) % 8
+        left[:, j * 256:j * 256 + 256] = normed[:, at((z + 8 + OFFSETS[slot]) % 8 * 256, 256)]
         for k, offset in enumerate(X_OFFSETS):
-            row = at(chunk * 256 + (x + 4 + offset) % 4 * 64, 64)
+            row = at(j * 256 + (x + 4 + offset) % 4 * 64, 64)
             unit, start = (units[k // 2], k % 2 * 64) if final else (units[j], k * 64)
             weights[row, :] = unit[start:start + 64, :]
-    if final:
-        lanes = at((z + 8 + OFFSETS[slots[0]]) % 8 * 256, 256)
-    else:
-        missing = at((z + 8 + OFFSETS[7]) % 8 * 256, 256)
-        weights[missing, :] = jnp.zeros((256, 1024), bf16)
 
     def columns(n, carry):
         part = at(n * 256, 256)
+        term = jnp.dot(left[...], weights[:, part], preferred_element_type=f32)
+        if not first:
+            term = term + before[:, part]
         if final:
-            term = before[:, part] + jnp.dot(normed[:, lanes], weights[:, part], preferred_element_type=f32)
             positive = jnp.maximum(term, 0.0)
-            out[:, part] = (positive * positive).astype(bf16)
-        else:
-            out[:, part] = jnp.dot(normed[...], weights[:, part], preferred_element_type=f32)
+            term = (positive * positive).astype(bf16)
+        out[:, part] = term
         return carry
 
     lax.fori_loop(0, 4, columns, 0)
@@ -369,8 +364,6 @@
         vmem=4,
     )
     up_units = z_ring(unit, 3)
-    far_up, far_down = half_of_each(up_units[5], up_units[6])
-    far_up, far_down = shift(far_up, Z, 1), shift(far_down, Z, -1)
     down_columns = call(
         functools.partial(gather_kernel, 32),
         jax.ShapeDtypeStruct((256, 2048), bf16),
@@ -381,8 +374,6 @@
         vmem=4,
     )
     before, after = shift(down_columns, X, 1), shift(down_columns, X, -1)
-    far_a, far_b = half_of_each(before, after)
-    far_a, far_b = shift(far_a, X, 1), shift(far_b, X, -1)
     docs = documents.reshape(1, -1)
     tokens = query_vectors.shape[0]
     pair = pltpu.VMEM((tokens, 128), bf16)
@@ -413,7 +404,7 @@
         functools.partial(gather_kernel, STATE_ROWS),
         jax.ShapeDtypeStruct((STATE_ROWS * (CHIPS_BACK + 1), 128), f32),
         [ANY] * (CHIPS_BACK + 1),
-        (state, *received),
+        lax.optimization_barrier((state, *received, down_columns))[:-1],
         scratch=[pltpu.SemaphoreType.DMA((CHIPS_BACK + 1,))],
         flops=1_000_000,
         vmem=4,
@@ -423,7 +414,7 @@
         early_kernel,
         jax.ShapeDtypeStruct((4, 128, 2048), bf16),
         [HBM] * 2,
-        (residual, w_out),
+        lax.optimization_barrier((residual, w_out, unit))[:2],
         scratch=[pltpu.SemaphoreType.DMA((8,))],
         flops=1_000_000,
         vmem=4,
@@ -461,23 +452,30 @@
         ],
         flops=2 * 512 * 512 * 2048,
     )
-    early_slots = tuple(range(7))
-    summed = call(
-        functools.partial(up_kernel, early_slots, False),
-        jax.ShapeDtypeStruct((512, 1024), f32),
-        [VM] * 8,
-        (normed, *up_units[:7]),
-        scratch=[pltpu.VMEM((2048, 1024), bf16)],
-        flops=2 * 512 * 1024 * 1792,
-    )
-    hidden = call(
-        functools.partial(up_kernel, (7,), True),
-        jax.ShapeDtypeStruct((512, 1024), bf16),
-        [VM] * 4,
-        (normed, far_up, far_down, summed),
-        scratch=[pltpu.VMEM((256, 1024), bf16)],
-        flops=2 * 512 * 1024 * 256,
-    )
+    ready = lax.optimization_barrier((before, after, normed))
+    far_a, far_b = half_of_each(ready[0], ready[1])
+    far_a, far_b, normed = lax.optimization_barrier((far_a, far_b, normed))
+    far_a, far_b = shift(far_a, X, 1), shift(far_b, X, -1)
+
+    def up(slots, units, summed, final=False):
+        return call(
+            functools.partial(up_kernel, slots, not summed, final),
+            jax.ShapeDtypeStruct((512, 1024), bf16 if final else f32),
+            [VM] * (1 + len(units) + len(summed)),
+            (normed, *units, *summed),
+            scratch=[
+                pltpu.VMEM((256 * len(slots), 1024), bf16),
+                pltpu.VMEM((512, 256 * len(slots)), bf16),
+            ],
+            flops=2 * 512 * 1024 * 256 * len(slots),
+        )
+
+    summed = up((0, 1, 2, 3, 4), up_units[:5], ())
+    ready = lax.optimization_barrier((up_units[5], up_units[6], normed))
+    far_up, far_down = half_of_each(ready[0], ready[1])
+    far_up, far_down = shift(far_up, Z, 1), shift(far_down, Z, -1)
+    summed = up((5, 6), up_units[5:7], (summed,))
+    hidden = up((7,), (far_up, far_down), (summed,), True)
     hidden_other = shift(hidden, C, 1)
     pieces = (down_columns, before, after, far_a, far_b)
     space = pltpu.VMEM((1024, 1024), bf16)

time: 199 us -> 174 us (0.87)
  waiting for transfers between devices: 112 us -> 73.3 us
  blocking collectives: 0 us -> 29.5 us
  starting transfers between devices: 62.7 us -> 46.9 us
    all_to_all x0 -> x1, blocking collectives: none -> 29.5 us  [layer(): early_own = lax.all_to_all(early, Y, 0, 0, tiled=True)]
    all_to_all x1 -> x0, waiting for transfers between devices: 26.2 us -> none  [layer(): early_own = lax.all_to_all(early, Y, 0, 0, tiled=True)]
    ppermute x4, waiting for transfers between devices: 14.2 us -> 2.12 us  [layer(): lax.ppermute(state, (Z, X), [(i, (i + back) % 32) for i in range(32)])]
    ppermute x4, starting transfers between devices: 12.3 us -> 4.25 us  [layer(): lax.ppermute(state, (Z, X), [(i, (i + back) % 32) for i in range(32)])]
    ppermute x10, waiting for transfers between devices: 12.7 us -> 18.6 us  [to_peer(): return lax.ppermute(value, (C, Y), pairs)]
    ppermute x27, waiting for transfers between devices: 58.4 us -> 52.7 us  [shift(): return lax.ppermute(value, axis, [(i, (i + by) % n) for i in range(n)])]
    all_to_all x1 -> x0, starting transfers between devices: 4.61 us -> none  [layer(): early_own = lax.all_to_all(early, Y, 0, 0, tiled=True)]
    ppermute x10, starting transfers between devices: 10.1 us -> 7.6 us  [to_peer(): return lax.ppermute(value, (C, Y), pairs)]
  transfers between devices with their start and end apart: 42 -> 41, of which waited for: 23 -> 24; matrix products, arithmetic and copies ran while one was open for 0% -> 0% of each run, Pallas kernels for 8% -> 8%
where the time goes in v1:
time: 174 us; the launch traced here: 173 us
  waiting for transfers between devices  73.3 us (42%)
  starting transfers between devices  46.9 us (27%)
  blocking collectives  29.5 us (17%)
  Pallas kernels  19.7 us (11%)
  local copies, waits for them, and re-layouts  2.04 us (1%)
    ppermute x27, waiting for transfers between devices, shift(): return lax.ppermute(value, axis, [(i, (i + by) % n) for i in range(n)])  52.7 us
    ppermute x27, starting transfers between devices, shift(): return lax.ppermute(value, axis, [(i, (i + by) % n) for i in range(n)])  35 us
    all_to_all x1, blocking collectives, layer(): early_own = lax.all_to_all(early, Y, 0, 0, tiled=True)  29.5 us
    pallas_call x16, Pallas kernels, call(): pl.pallas_call(kernel, out_shape=outs, in_specs=ins, out_specs=[VM] * len...  19.7 us
    ppermute x10, waiting for transfers between devices, to_peer(): return lax.ppermute(value, (C, Y), pairs)  18.6 us
    ppermute x10, starting transfers between devices, to_peer(): return lax.ppermute(value, (C, Y), pairs)  7.6 us
    ppermute x4, starting transfers between devices, layer(): lax.ppermute(state, (Z, X), [(i, (i + back) % 32) for i in range(32)])  4.25 us
  transfers between devices with their start and end apart: 41, of which 24 were waited for; matrix products, arithmetic and copies ran while one was open for 0% of the time, Pallas kernels for 8%

profile of v1, /device:TPU:2, one launch (start us, length us, event | category | flops | bytes accessed | tf_op | source)
XLA Modules:
  0.0 172.7 jit_solution(2190524169771074091)
XLA Ops:
  1.0 1.2 collective-permute-done
  2.3 1.6 collective-permute-start.1
  4.7 2.0 %collective-permute-start.3 = (bf16[64,1024]{1,0:T(8,128)(2,1)S(1)}, bf16[64,1024]{1,0:T(8,128)(2,1)S(1)}, u32[]{:S(2)}, u32[]{:S(2)}) collective-permute-start(bf16[64,1024]{1,0:T(8,128)(2,1)S(1)} %maximum_select_fusion.refs_0_), channel_id=1, source_target_pairs={{0,16},{8,24},{16,0},{24,8},{1,17},{9,25},{17,1},{25,9},{2,18},{10... | collective-permute-start | bytes 393224 | tf_op jit(solution)/shard_map/ppermute | solution.py:300
  6.6 1.9 %collective-permute-done.1.refs_1_ = bf16[64,1024]{1,0:T(8,128)(2,1)S(1)} collective-permute-done((bf16[64,1024]{1,0:T(8,128)(2,1)S(1)}, bf16[64,1024]{1,0:T(8,128)(2,1)S(1)}, u32[]{:S(2)}, u32[]{:S(2)}) %collective-permute-start.1) | collective-permute-done | bytes 131104 | tf_op jit(solution)/shard_map/ppermute | solution.py:300
  9.1 3.9 %collective-permute-done.3.refs_3_ = bf16[64,1024]{1,0:T(8,128)(2,1)S(1)} collective-permute-done((bf16[64,1024]{1,0:T(8,128)(2,1)S(1)}, bf16[64,1024]{1,0:T(8,128)(2,1)S(1)}, u32[]{:S(2)}, u32[]{:S(2)}) %collective-permute-start.3) | collective-permute-done | bytes 131104 | tf_op jit(solution)/shard_map/ppermute | solution.py:300
  13.7 1.0 copy-done
  16.0 29.5 %all_to_all.5.early_own = bf16[4,128,2048]{2,1,0:T(8,128)(2,1)S(1)} all-to-all(bf16[4,128,2048]{2,1,0:T(8,128)(2,1)S(1)} %shard_map.110), channel_id=1, replica_groups=mesh['sp_0'=8,'sp_1'=4,'sp_2'=2,'tp'=4] {'tp'}, dimensions={0} | all-to-all | bytes 4194304 | tf_op jit(solution)/shard_map/all_to_all | solution.py:422
  45.5 1.9 %collective-permute-start.9 = (bf16[32,2048]{1,0:T(8,128)(2,1)S(1)}, bf16[32,2048]{1,0:T(8,128)(2,1)S(1)}, u32[]{:S(2)}, u32[]{:S(2)}) collective-permute-start(bf16[32,2048]{1,0:T(8,128)(2,1)S(1)} %bitcast.2), channel_id=1, source_target_pairs={{0,32},{32,64},{64,96},{96,128},{128,160},{160,192},{192,224},{224... | collective-permute-start | bytes 393224 | tf_op jit(solution)/shard_map/ppermute | solution.py:300
  47.4 4.0 %collective-permute-start.10 = (bf16[32,2048]{1,0:T(8,128)(2,1)S(1)}, bf16[32,2048]{1,0:T(8,128)(2,1)S(1)}, u32[]{:S(2)}, u32[]{:S(2)}) collective-permute-start(bf16[32,2048]{1,0:T(8,128)(2,1)S(1)} %bitcast.3), channel_id=1, source_target_pairs={{0,224},{32,0},{64,32},{96,64},{128,96},{160,128},{192,160},{224,1... | collective-permute-start | bytes 393224 | tf_op jit(solution)/shard_map/ppermute | solution.py:300
  51.4 4.1 %collective-permute-done.9.refs_1_ = bf16[32,2048]{1,0:T(8,128)(2,1)S(1)} collective-permute-done((bf16[32,2048]{1,0:T(8,128)(2,1)S(1)}, bf16[32,2048]{1,0:T(8,128)(2,1)S(1)}, u32[]{:S(2)}, u32[]{:S(2)}) %collective-permute-start.9) | collective-permute-done | bytes 131104 | tf_op jit(solution)/shard_map/ppermute | solution.py:300
  55.5 3.2 %collective-permute-start.12 = (bf16[32,2048]{1,0:T(8,128)(2,1)S(1)}, bf16[32,2048]{1,0:T(8,128)(2,1)S(1)}, u32[]{:S(2)}, u32[]{:S(2)}) collective-permute-start(bf16[32,2048]{1,0:T(8,128)(2,1)S(1)} %collective-permute-done.10.refs_2_), channel_id=1, source_target_pairs={{0,224},{32,0},{64,32},{96,64},{128,96},{160,128},{192,160},{224,1... | collective-permute-start | bytes 393224 | tf_op jit(solution)/shard_map/ppermute | solution.py:300
  58.7 3.3 %collective-permute-done.11.refs_3_ = bf16[32,2048]{1,0:T(8,128)(2,1)S(1)} collective-permute-done((bf16[32,2048]{1,0:T(8,128)(2,1)S(1)}, bf16[32,2048]{1,0:T(8,128)(2,1)S(1)}, u32[]{:S(2)}, u32[]{:S(2)}) %collective-permute-start.11) | collective-permute-done | bytes 131104 | tf_op jit(solution)/shard_map/ppermute | solution.py:300
  62.0 3.2 %collective-permute-start.14 = (bf16[32,2048]{1,0:T(8,128)(2,1)S(1)}, bf16[32,2048]{1,0:T(8,128)(2,1)S(1)}, u32[]{:S(2)}, u32[]{:S(2)}) collective-permute-start(bf16[32,2048]{1,0:T(8,128)(2,1)S(1)} %collective-permute-done.12.refs_4_), channel_id=1, source_target_pairs={{0,224},{32,0},{64,32},{96,64},{128,96},{160,128},{192,160},{224,1... | collective-permute-start | bytes 393224 | tf_op jit(solution)/shard_map/ppermute | solution.py:300
  65.3 2.9 %collective-permute-done.13.refs_5_ = bf16[32,2048]{1,0:T(8,128)(2,1)S(1)} collective-permute-done((bf16[32,2048]{1,0:T(8,128)(2,1)S(1)}, bf16[32,2048]{1,0:T(8,128)(2,1)S(1)}, u32[]{:S(2)}, u32[]{:S(2)}) %collective-permute-start.13) | collective-permute-done | bytes 131104 | tf_op jit(solution)/shard_map/ppermute | solution.py:300
  68.3 2.2 %shard_map.111 = (f32[72,128]{1,0:T(8,128)S(1)}, f32[256,768]{1,0:T(8,128)S(1)}) custom-call(f32[2,256]{1,0:T(2,128)S(1)} %copy-done.6, f32[2,256]{1,0:T(2,128)S(1)} %copy-done.7, s32[1,256]{1,0:T(1,128)S(1)} %bitcast.5, bf16[256,128]{1,0:T(8,128)(2,1)S(1)} %copy-done.3, bf16[256,128]{1,0:T(8,128)(2,1)S(1)} %copy-done.4, bf16[256,128]{1,0:T(8,128)(2,1)S(1)} %copy-done.5), custom_call_target="tpu_custom_call" | custom-call | flops 150000000 | bytes 1 | tf_op jit(solution)/shard_map/pallas_call | solution.py:30
  70.5 1.6 collective-permute-start.6
  72.9 1.5 collective-permute-done.15.refs_7_
  74.4 1.8 %collective-permute-start.8 = (f32[72,128]{1,0:T(8,128)S(1)}, f32[72,128]{1,0:T(8,128)S(1)}, u32[]{:S(2)}, u32[]{:S(2)}) collective-permute-start(f32[72,128]{1,0:T(8,128)S(1)} %get-tuple-element.39.refs_0_), channel_id=1, source_target_pairs={{0,32},{8,40},{16,48},{24,56},{32,64},{40,72},{48,80},{56,88},{64,... | collective-permute-start | bytes 110600 | tf_op jit(solution)/shard_map/ppermute | solution.py:400
  76.2 1.4 shard_map.112.mine
  78.6 1.1 collective-permute-done.8.refs_4_
  80.1 1.8 %collective-permute-start.23 = (bf16[256,1024]{1,0:T(8,128)(2,1)S(1)}, bf16[256,1024]{1,0:T(8,128)(2,1)S(1)}, u32[]{:S(2)}, u32[]{:S(2)}) collective-permute-start(bf16[256,1024]{1,0:T(8,128)(2,1)S(1)} %shard_map.109.refs_0_), channel_id=1, source_target_pairs={{0,32},{32,64},{64,96},{96,128},{128,160},{160,192},{192,224},{224... | collective-permute-start | bytes 1572872 | tf_op jit(solution)/shard_map/ppermute | solution.py:300
  81.9 1.5 collective-permute-start.26
  84.5 2.1 %collective-permute-start.18 = (bf16[256,128]{1,0:T(8,128)(2,1)S(1)}, bf16[256,128]{1,0:T(8,128)(2,1)S(1)}, u32[]{:S(2)}, u32[]{:S(2)}) collective-permute-start(bf16[256,128]{1,0:T(8,128)(2,1)S(1)} %shard_map.114.refs_0_), channel_id=1, source_target_pairs={{0,2},{1,3},{2,0},{3,1},{4,6},{5,7},{6,4},{7,5},{8,10},{9,11},{10,... | collective-permute-start | bytes 196616 | tf_op jit(solution)/shard_map/ppermute | solution.py:305
  86.5 4.0 %collective-permute-done.17.refs_1_ = bf16[256,128]{1,0:T(8,128)(2,1)S(1)} collective-permute-done((bf16[256,128]{1,0:T(8,128)(2,1)S(1)}, bf16[256,128]{1,0:T(8,128)(2,1)S(1)}, u32[]{:S(2)}, u32[]{:S(2)}) %collective-permute-start.17) | collective-permute-done | bytes 65568 | tf_op jit(solution)/shard_map/ppermute | solution.py:305
  90.5 4.3 %collective-permute-done.19.refs_3_ = bf16[256,128]{1,0:T(8,128)(2,1)S(1)} collective-permute-done((bf16[256,128]{1,0:T(8,128)(2,1)S(1)}, bf16[256,128]{1,0:T(8,128)(2,1)S(1)}, u32[]{:S(2)}, u32[]{:S(2)}) %collective-permute-start.19) | collective-permute-done | bytes 65568 | tf_op jit(solution)/shard_map/ppermute | solution.py:305
  95.2 2.4 %collective-permute-start.21 = (bf16[256,2048]{1,0:T(8,128)(2,1)S(1)}, bf16[256,2048]{1,0:T(8,128)(2,1)S(1)}, u32[]{:S(2)}, u32[]{:S(2)}) collective-permute-start(bf16[256,2048]{1,0:T(8,128)(2,1)S(1)} %shard_map.112.mine), channel_id=1, source_target_pairs={{0,8},{8,16},{16,24},{24,0},{1,9},{9,17},{17,25},{25,1},{2,10},{10... | collective-permute-start | bytes 3145736 | tf_op jit(solution)/shard_map/ppermute | solution.py:300
  97.6 1.2 collective-permute-start.24
  98.8 2.1 %collective-permute-start.27 = (bf16[256,1024]{1,0:T(8,128)(2,1)S(1)}, bf16[256,1024]{1,0:T(8,128)(2,1)S(1)}, u32[]{:S(2)}, u32[]{:S(2)}) collective-permute-start(bf16[256,1024]{1,0:T(8,128)(2,1)S(1)} %collective-permute-done.26.refs_2_), channel_id=1, source_target_pairs={{0,224},{32,0},{64,32},{96,64},{128,96},{160,128},{192,160},{224,1... | collective-permute-start | bytes 1572872 | tf_op jit(solution)/shard_map/ppermute | solution.py:300
  100.9 11.9 %collective-permute-done.24.refs_3_ = bf16[256,1024]{1,0:T(8,128)(2,1)S(1)} collective-permute-done((bf16[256,1024]{1,0:T(8,128)(2,1)S(1)}, bf16[256,1024]{1,0:T(8,128)(2,1)S(1)}, u32[]{:S(2)}, u32[]{:S(2)}) %collective-permute-start.24) | collective-permute-done | bytes 524320 | tf_op jit(solution)/shard_map/ppermute | solution.py:300
  112.9 3.2 %collective-permute-start.28 = (bf16[256,1024]{1,0:T(8,128)(2,1)S(1)}, bf16[256,1024]{1,0:T(8,128)(2,1)S(1)}, u32[]{:S(2)}, u32[]{:S(2)}) collective-permute-start(bf16[256,1024]{1,0:T(8,128)(2,1)S(1)} %collective-permute-done.27.refs_4_), channel_id=1, source_target_pairs={{0,224},{32,0},{64,32},{96,64},{128,96},{160,128},{192,160},{224,1... | collective-permute-start | bytes 1572872 | tf_op jit(solution)/shard_map/ppermute | solution.py:300
  116.1 3.4 %shard_map.116 = (bf16[512,2048]{1,0:T(8,128)(2,1)S(1)}, bf16[512,2048]{1,0:T(8,128)(2,1)S(1)}) custom-call(bf16[4,128,2048]{2,1,0:T(8,128)(2,1)S(1)} %all_to_all.5.early_own, bf16[4,128,2048]{2,1,0:T(8,128)(2,1)S(1)} %collective-permute-done.4.early_other, bf16[1,2048]{1,0:T(2,128)(2,1)S(1)} %reshape.6.gain, bf16[1024,128]{1,0:T(8,128)(2,1)S(1)} %shard_map.115.mixes_own, ...), custom_call_target="tpu_custom_call" | custom-call | flops 1073741824 | bytes 1 | tf_op jit(solution)/shard_map/pallas_call | solution.py:30
  119.6 1.3 collective-permute-done.21.one.before
  120.8 2.0 %collective-permute-done.22.two.after = bf16[256,2048]{1,0:T(8,128)(2,1)S(1)} collective-permute-done((bf16[256,2048]{1,0:T(8,128)(2,1)S(1)}, bf16[256,2048]{1,0:T(8,128)(2,1)S(1)}, u32[]{:S(2)}, u32[]{:S(2)}) %collective-permute-start.22) | collective-permute-done | bytes 1048608 | tf_op jit(solution)/shard_map/ppermute | solution.py:300
  122.9 4.3 %collective-permute-done.25.one.refs_0_ = bf16[256,1024]{1,0:T(8,128)(2,1)S(1)} collective-permute-done((bf16[256,1024]{1,0:T(8,128)(2,1)S(1)}, bf16[256,1024]{1,0:T(8,128)(2,1)S(1)}, u32[]{:S(2)}, u32[]{:S(2)}) %collective-permute-start.25) | collective-permute-done | bytes 524320 | tf_op jit(solution)/shard_map/ppermute | solution.py:300
  127.6 3.2 %collective-permute-start.30 = (bf16[128,1024]{1,0:T(8,128)(2,1)S(1)}, bf16[128,1024]{1,0:T(8,128)(2,1)S(1)}, u32[]{:S(2)}, u32[]{:S(2)}) collective-permute-start(bf16[128,1024]{1,0:T(8,128)(2,1)S(1)} %get-tuple-element.54), channel_id=1, source_target_pairs={{0,224},{32,0},{64,32},{96,64},{128,96},{160,128},{192,160},{224,1... | collective-permute-start | bytes 786440 | tf_op jit(solution)/shard_map/ppermute | solution.py:300
  130.8 2.5 %shard_map.119.refs_2_ = f32[512,1024]{1,0:T(8,128)S(1)} custom-call(bf16[512,2048]{1,0:T(8,128)(2,1)S(1)} %get-tuple-element.50.normed, bf16[256,1024]{1,0:T(8,128)(2,1)S(1)} %shard_map.109.refs_0_, bf16[256,1024]{1,0:T(8,128)(2,1)S(1)} %collective-permute-done.23.refs_1_, bf16[256,1024]{1,0:T(8,128)(2,1)S(1)} %collective-permute-done.26.refs_2_, ...), custom_call_target="tpu_custom_call" | custom-call | flops 1342177280 | bytes 1 | tf_op jit(solution)/shard_map/pallas_call | solution.py:30
  133.3 1.4 shard_map.120.refs_2_
  135.4 1.0 shard_map.121.hidden
  136.5 1.2 collective-permute-start.32
  138.7 12.2 %collective-permute-done.32.far_a = bf16[128,2048]{1,0:T(8,128)(2,1)S(1)} collective-permute-done((bf16[128,2048]{1,0:T(8,128)(2,1)S(1)}, bf16[128,2048]{1,0:T(8,128)(2,1)S(1)}, u32[]{:S(2)}, u32[]{:S(2)}) %collective-permute-start.32) | collective-permute-done | bytes 524320 | tf_op jit(solution)/shard_map/ppermute | solution.py:300
  151.7 2.0 %shard_map.122.refs_0_ = f32[512,1024]{1,0:T(8,128)S(1)} custom-call(bf16[512,1024]{1,0:T(8,128)(2,1)S(1)} %shard_map.121.hidden, bf16[256,2048]{1,0:T(8,128)(2,1)S(1)} %shard_map.112.mine, bf16[256,2048]{1,0:T(8,128)(2,1)S(1)} %collective-permute-done.21.one.before, bf16[256,2048]{1,0:T(8,128)(2,1)S(1)} %collective-permute-done.22.two.after, ...), custom_call_target="tpu_custom_call" | custom-call | flops 1073741824 | bytes 1 | tf_op jit(solution)/shard_map/pallas_call | solution.py:30
  153.8 2.2 %shard_map.123 = (bf16[64,1024]{1,0:T(8,128)(2,1)S(1)}, bf16[64,1024]{1,0:T(8,128)(2,1)S(1)}, bf16[64,1024]{1,0:T(8,128)(2,1)S(1)}, bf16[64,1024]{1,0:T(8,128)(2...) custom-call(bf16[512,1024]{1,0:T(8,128)(2,1)S(1)} %collective-permut, ...), custom_call_target="tpu_custom_call" | custom-call | flops 1073741824 | bytes 1 | tf_op jit(solution)/shard_map/pallas_call | solution.py:30
  156.0 2.7 %collective-permute-start.35 = (bf16[64,1024]{1,0:T(8,128)(2,1)S(1)}, bf16[64,1024]{1,0:T(8,128)(2,1)S(1)}, u32[]{:S(2)}, u32[]{:S(2)}) collective-permute-start(bf16[64,1024]{1,0:T(8,128)(2,1)S(1)} %get-tuple-element.59), channel_id=1, source_target_pairs={{0,2},{1,3},{2,0},{3,1},{4,6},{5,7},{6,4},{7,5},{8,10},{9,11},{10,... | collective-permute-start | bytes 393224 | tf_op jit(solution)/shard_map/ppermute | solution.py:305
  159.3 1.6 collective-permute-start.38
  160.8 4.4 %collective-permute-done.34.refs_1_ = bf16[64,1024]{1,0:T(8,128)(2,1)S(1)} collective-permute-done((bf16[64,1024]{1,0:T(8,128)(2,1)S(1)}, bf16[64,1024]{1,0:T(8,128)(2,1)S(1)}, u32[]{:S(2)}, u32[]{:S(2)}) %collective-permute-start.34) | collective-permute-done | bytes 131104 | tf_op jit(solution)/shard_map/ppermute | solution.py:305
  165.3 1.6 collective-permute-done.38.refs_5_
  167.0 4.2 %collective-permute-done.39.refs_6_ = bf16[64,1024]{1,0:T(8,128)(2,1)S(1)} collective-permute-done((bf16[64,1024]{1,0:T(8,128)(2,1)S(1)}, bf16[64,1024]{1,0:T(8,128)(2,1)S(1)}, u32[]{:S(2)}, u32[]{:S(2)}) %collective-permute-start.39) | collective-permute-done | bytes 131104 | tf_op jit(solution)/shard_map/ppermute | solution.py:305
  171.2 1.5 shard_map.124
  (74 shorter events, 11.9 us)
Async XLA Ops:
  0.9 1.3 collective-permute-start
  2.3 6.3 %collective-permute-start.1 = (bf16[64,1024]{1,0:T(8,128)(2,1)S(1)}, bf16[64,1024]{1,0:T(8,128)(2,1)S(1)}, u32[]{:S(2)}, u32[]{:S(2)}) collective-permute-start(bf16[64,1024]{1,0:T(8,128)(2,1)S(1)} %maximum_select_fusion.refs_0_), channel_id=1, source_target_pairs={{0,8},{8,16},{16,24},{24,0},{1,9},{9,17},{17,25},{25,1},{2,10},{10... | collective-permute-start | bytes 393224 | tf_op jit(solution)/shard_map/ppermute | solution.py:300
  3.8 5.3 %collective-permute-start.2 = (bf16[64,1024]{1,0:T(8,128)(2,1)S(1)}, bf16[64,1024]{1,0:T(8,128)(2,1)S(1)}, u32[]{:S(2)}, u32[]{:S(2)}) collective-permute-start(bf16[64,1024]{1,0:T(8,128)(2,1)S(1)} %maximum_select_fusion.refs_0_), channel_id=1, source_target_pairs={{0,24},{8,0},{16,8},{24,16},{1,25},{9,1},{17,9},{25,17},{2,26},{10... | collective-permute-start | bytes 393224 | tf_op jit(solution)/shard_map/ppermute | solution.py:300
  4.7 8.3 %collective-permute-start.3 = (bf16[64,1024]{1,0:T(8,128)(2,1)S(1)}, bf16[64,1024]{1,0:T(8,128)(2,1)S(1)}, u32[]{:S(2)}, u32[]{:S(2)}) collective-permute-start(bf16[64,1024]{1,0:T(8,128)(2,1)S(1)} %maximum_select_fusion.refs_0_), channel_id=1, source_target_pairs={{0,16},{8,24},{16,0},{24,8},{1,17},{9,25},{17,1},{25,9},{2,18},{10... | collective-permute-start | bytes 393224 | tf_op jit(solution)/shard_map/ppermute | solution.py:300
  15.9 52.3 %copy-start.3 = (bf16[256,128]{1,0:T(8,128)(2,1)S(1)}, bf16[256,128]{1,0:T(8,128)(2,1)}, u32[]{:S(2)}) copy-start(bf16[256,128]{1,0:T(8,128)(2,1)} %refs_3_.1) | copy-start | bytes 196612
  15.9 52.3 %copy-start.4 = (bf16[256,128]{1,0:T(8,128)(2,1)S(1)}, bf16[256,128]{1,0:T(8,128)(2,1)}, u32[]{:S(2)}) copy-start(bf16[256,128]{1,0:T(8,128)(2,1)} %refs_4_.1) | copy-start | bytes 196612
  16.0 52.3 %copy-start.5 = (bf16[256,128]{1,0:T(8,128)(2,1)S(1)}, bf16[256,128]{1,0:T(8,128)(2,1)}, u32[]{:S(2)}) copy-start(bf16[256,128]{1,0:T(8,128)(2,1)} %refs_5_.1) | copy-start | bytes 196612
  16.0 52.3 %copy-start.6 = (f32[2,256]{1,0:T(2,128)S(1)}, f32[2,256]{1,0:T(2,128)}, u32[]{:S(2)}) copy-start(f32[2,256]{1,0:T(2,128)} %refs_0_.1) | copy-start | bytes 6148
  16.0 52.3 %copy-start.7 = (f32[2,256]{1,0:T(2,128)S(1)}, f32[2,256]{1,0:T(2,128)}, u32[]{:S(2)}) copy-start(f32[2,256]{1,0:T(2,128)} %refs_1_.1) | copy-start | bytes 6148
  16.0 52.3 %copy-start.8 = (s32[256]{0:T(256)S(1)}, s32[256]{0:T(256)}, u32[]{:S(2)}) copy-start(s32[256]{0:T(256)} %param.17) | copy-start | bytes 3076
  45.5 70.7 %collective-permute-start.4 = (bf16[4,128,2048]{2,1,0:T(8,128)(2,1)S(1)}, bf16[4,128,2048]{2,1,0:T(8,128)(2,1)S(1)}, u32[]{:S(2)}, u32[]{:S(2)}) collective-permute-start(bf16[4,128,2048]{2,1,0:T(8,128)(2,1)S(1)} %all_to_all.5.early_own), channel_id=1, source_target_pairs={{0,4},{4,0},{1,5},{5,1},{2,6},{6,2},{3,7},{7,3},{8,12},{12,8},{9,1... | collective-permute-start | bytes 6291464 | tf_op jit(solution)/shard_map/ppermute | solution.py:300
  45.5 10.0 %collective-permute-start.9 = (bf16[32,2048]{1,0:T(8,128)(2,1)S(1)}, bf16[32,2048]{1,0:T(8,128)(2,1)S(1)}, u32[]{:S(2)}, u32[]{:S(2)}) collective-permute-start(bf16[32,2048]{1,0:T(8,128)(2,1)S(1)} %bitcast.2), channel_id=1, source_target_pairs={{0,32},{32,64},{64,96},{96,128},{128,160},{160,192},{192,224},{224... | collective-permute-start | bytes 393224 | tf_op jit(solution)/shard_map/ppermute | solution.py:300
  47.4 8.1 %collective-permute-start.10 = (bf16[32,2048]{1,0:T(8,128)(2,1)S(1)}, bf16[32,2048]{1,0:T(8,128)(2,1)S(1)}, u32[]{:S(2)}, u32[]{:S(2)}) collective-permute-start(bf16[32,2048]{1,0:T(8,128)(2,1)S(1)} %bitcast.3), channel_id=1, source_target_pairs={{0,224},{32,0},{64,32},{96,64},{128,96},{160,128},{192,160},{224,1... | collective-permute-start | bytes 393224 | tf_op jit(solution)/shard_map/ppermute | solution.py:300
  55.5 6.5 %collective-permute-start.11 = (bf16[32,2048]{1,0:T(8,128)(2,1)S(1)}, bf16[32,2048]{1,0:T(8,128)(2,1)S(1)}, u32[]{:S(2)}, u32[]{:S(2)}) collective-permute-start(bf16[32,2048]{1,0:T(8,128)(2,1)S(1)} %collective-permute-done.9.refs_1_), channel_id=1, source_target_pairs={{0,32},{32,64},{64,96},{96,128},{128,160},{160,192},{192,224},{224... | collective-permute-start | bytes 393224 | tf_op jit(solution)/shard_map/ppermute | solution.py:300
  55.5 6.5 %collective-permute-start.12 = (bf16[32,2048]{1,0:T(8,128)(2,1)S(1)}, bf16[32,2048]{1,0:T(8,128)(2,1)S(1)}, u32[]{:S(2)}, u32[]{:S(2)}) collective-permute-start(bf16[32,2048]{1,0:T(8,128)(2,1)S(1)} %collective-permute-done.10.refs_2_), channel_id=1, source_target_pairs={{0,224},{32,0},{64,32},{96,64},{128,96},{160,128},{192,160},{224,1... | collective-permute-start | bytes 393224 | tf_op jit(solution)/shard_map/ppermute | solution.py:300
  62.0 6.2 %collective-permute-start.13 = (bf16[32,2048]{1,0:T(8,128)(2,1)S(1)}, bf16[32,2048]{1,0:T(8,128)(2,1)S(1)}, u32[]{:S(2)}, u32[]{:S(2)}) collective-permute-start(bf16[32,2048]{1,0:T(8,128)(2,1)S(1)} %collective-permute-done.11.refs_3_), channel_id=1, source_target_pairs={{0,32},{32,64},{64,96},{96,128},{128,160},{160,192},{192,224},{224... | collective-permute-start | bytes 393224 | tf_op jit(solution)/shard_map/ppermute | solution.py:300
  62.0 10.1 %collective-permute-start.14 = (bf16[32,2048]{1,0:T(8,128)(2,1)S(1)}, bf16[32,2048]{1,0:T(8,128)(2,1)S(1)}, u32[]{:S(2)}, u32[]{:S(2)}) collective-permute-start(bf16[32,2048]{1,0:T(8,128)(2,1)S(1)} %collective-permute-done.12.refs_4_), channel_id=1, source_target_pairs={{0,224},{32,0},{64,32},{96,64},{128,96},{160,128},{192,160},{224,1... | collective-permute-start | bytes 393224 | tf_op jit(solution)/shard_map/ppermute | solution.py:300
  68.2 6.2 %collective-permute-start.15 = (bf16[32,2048]{1,0:T(8,128)(2,1)S(1)}, bf16[32,2048]{1,0:T(8,128)(2,1)S(1)}, u32[]{:S(2)}, u32[]{:S(2)}) collective-permute-start(bf16[32,2048]{1,0:T(8,128)(2,1)S(1)} %collective-permute-done.13.refs_5_), channel_id=1, source_target_pairs={{0,32},{32,64},{64,96},{96,128},{128,160},{160,192},{192,224},{224... | collective-permute-start | bytes 393224 | tf_op jit(solution)/shard_map/ppermute | solution.py:300
  70.4 45.7 %copy-start.9 = (bf16[2048]{0:T(1024)(128)(2,1)S(1)}, bf16[2048]{0:T(1024)(128)(2,1)}, u32[]{:S(2)}) copy-start(bf16[2048]{0:T(1024)(128)(2,1)} %param.19) | copy-start | bytes 12292
  70.5 7.1 %collective-permute-start.5 = (f32[72,128]{1,0:T(8,128)S(1)}, f32[72,128]{1,0:T(8,128)S(1)}, u32[]{:S(2)}, u32[]{:S(2)}) collective-permute-start(f32[72,128]{1,0:T(8,128)S(1)} %get-tuple-element.39.refs_0_), channel_id=1, source_target_pairs={{0,8},{8,16},{16,24},{24,32},{32,40},{40,48},{48,56},{56,64},{64,7... | collective-permute-start | bytes 110600 | tf_op jit(solution)/shard_map/ppermute | solution.py:400
  70.5 7.8 %collective-permute-start.6 = (f32[72,128]{1,0:T(8,128)S(1)}, f32[72,128]{1,0:T(8,128)S(1)}, u32[]{:S(2)}, u32[]{:S(2)}) collective-permute-start(f32[72,128]{1,0:T(8,128)S(1)} %get-tuple-element.39.refs_0_), channel_id=1, source_target_pairs={{0,16},{8,24},{16,32},{24,40},{32,48},{40,56},{48,64},{56,72},{64,... | collective-permute-start | bytes 110600 | tf_op jit(solution)/shard_map/ppermute | solution.py:400
  72.2 6.4 %collective-permute-start.7 = (f32[72,128]{1,0:T(8,128)S(1)}, f32[72,128]{1,0:T(8,128)S(1)}, u32[]{:S(2)}, u32[]{:S(2)}) collective-permute-start(f32[72,128]{1,0:T(8,128)S(1)} %get-tuple-element.39.refs_0_), channel_id=1, source_target_pairs={{0,24},{8,32},{16,40},{24,48},{32,56},{40,64},{48,72},{56,80},{64,... | collective-permute-start | bytes 110600 | tf_op jit(solution)/shard_map/ppermute | solution.py:400
  74.4 5.3 %collective-permute-start.8 = (f32[72,128]{1,0:T(8,128)S(1)}, f32[72,128]{1,0:T(8,128)S(1)}, u32[]{:S(2)}, u32[]{:S(2)}) collective-permute-start(f32[72,128]{1,0:T(8,128)S(1)} %get-tuple-element.39.refs_0_), channel_id=1, source_target_pairs={{0,32},{8,40},{16,48},{24,56},{32,64},{40,72},{48,80},{56,88},{64,... | collective-permute-start | bytes 110600 | tf_op jit(solution)/shard_map/ppermute | solution.py:400
  80.0 3.4 %collective-permute-start.16 = (f32[360,128]{1,0:T(8,128)S(1)}, f32[360,128]{1,0:T(8,128)S(1)}, u32[]{:S(2)}, u32[]{:S(2)}) collective-permute-start(f32[360,128]{1,0:T(8,128)S(1)} %shard_map.113.states_own), channel_id=1, source_target_pairs={{0,4},{4,0},{1,5},{5,1},{2,6},{6,2},{3,7},{7,3},{8,12},{12,8},{9,1... | collective-permute-start | bytes 552968 | tf_op jit(solution)/shard_map/ppermute | solution.py:300
  80.1 17.5 %collective-permute-start.23 = (bf16[256,1024]{1,0:T(8,128)(2,1)S(1)}, bf16[256,1024]{1,0:T(8,128)(2,1)S(1)}, u32[]{:S(2)}, u32[]{:S(2)}) collective-permute-start(bf16[256,1024]{1,0:T(8,128)(2,1)S(1)} %shard_map.109.refs_0_), channel_id=1, source_target_pairs={{0,32},{32,64},{64,96},{96,128},{128,160},{160,192},{192,224},{224... | collective-permute-start | bytes 1572872 | tf_op jit(solution)/shard_map/ppermute | solution.py:300
  81.9 15.7 %collective-permute-start.26 = (bf16[256,1024]{1,0:T(8,128)(2,1)S(1)}, bf16[256,1024]{1,0:T(8,128)(2,1)S(1)}, u32[]{:S(2)}, u32[]{:S(2)}) collective-permute-start(bf16[256,1024]{1,0:T(8,128)(2,1)S(1)} %shard_map.109.refs_0_), channel_id=1, source_target_pairs={{0,224},{32,0},{64,32},{96,64},{128,96},{160,128},{192,160},{224,1... | collective-permute-start | bytes 1572872 | tf_op jit(solution)/shard_map/ppermute | solution.py:300
  83.8 6.7 %collective-permute-start.17 = (bf16[256,128]{1,0:T(8,128)(2,1)S(1)}, bf16[256,128]{1,0:T(8,128)(2,1)S(1)}, u32[]{:S(2)}, u32[]{:S(2)}) collective-permute-start(bf16[256,128]{1,0:T(8,128)(2,1)S(1)} %shard_map.114.refs_0_), channel_id=1, source_target_pairs={{0,1},{1,2},{2,3},{3,0},{4,5},{5,6},{6,7},{7,4},{8,9},{9,10},{10,1... | collective-permute-start | bytes 196616 | tf_op jit(solution)/shard_map/ppermute | solution.py:305
  84.5 6.1 %collective-permute-start.18 = (bf16[256,128]{1,0:T(8,128)(2,1)S(1)}, bf16[256,128]{1,0:T(8,128)(2,1)S(1)}, u32[]{:S(2)}, u32[]{:S(2)}) collective-permute-start(bf16[256,128]{1,0:T(8,128)(2,1)S(1)} %shard_map.114.refs_0_), channel_id=1, source_target_pairs={{0,2},{1,3},{2,0},{3,1},{4,6},{5,7},{6,4},{7,5},{8,10},{9,11},{10,... | collective-permute-start | bytes 196616 | tf_op jit(solution)/shard_map/ppermute | solution.py:305
  90.5 4.3 %collective-permute-start.19 = (bf16[256,128]{1,0:T(8,128)(2,1)S(1)}, bf16[256,128]{1,0:T(8,128)(2,1)S(1)}, u32[]{:S(2)}, u32[]{:S(2)}) collective-permute-start(bf16[256,128]{1,0:T(8,128)(2,1)S(1)} %shard_map.114.refs_0_), channel_id=1, source_target_pairs={{0,3},{1,0},{2,1},{3,2},{4,7},{5,4},{6,5},{7,6},{8,11},{9,8},{10,9... | collective-permute-start | bytes 196616 | tf_op jit(solution)/shard_map/ppermute | solution.py:305
  95.1 3.7 %collective-permute-start.20 = (bf16[1024,128]{1,0:T(8,128)(2,1)S(1)}, bf16[1024,128]{1,0:T(8,128)(2,1)S(1)}, u32[]{:S(2)}, u32[]{:S(2)}) collective-permute-start(bf16[1024,128]{1,0:T(8,128)(2,1)S(1)} %shard_map.115.mixes_own), channel_id=1, source_target_pairs={{0,4},{4,0},{1,5},{5,1},{2,6},{6,2},{3,7},{7,3},{8,12},{12,8},{9,1... | collective-permute-start | bytes 786440 | tf_op jit(solution)/shard_map/ppermute | solution.py:300
  95.2 25.6 %collective-permute-start.21 = (bf16[256,2048]{1,0:T(8,128)(2,1)S(1)}, bf16[256,2048]{1,0:T(8,128)(2,1)S(1)}, u32[]{:S(2)}, u32[]{:S(2)}) collective-permute-start(bf16[256,2048]{1,0:T(8,128)(2,1)S(1)} %shard_map.112.mine), channel_id=1, source_target_pairs={{0,8},{8,16},{16,24},{24,0},{1,9},{9,17},{17,25},{25,1},{2,10},{10... | collective-permute-start | bytes 3145736 | tf_op jit(solution)/shard_map/ppermute | solution.py:300
  97.6 25.2 %collective-permute-start.22 = (bf16[256,2048]{1,0:T(8,128)(2,1)S(1)}, bf16[256,2048]{1,0:T(8,128)(2,1)S(1)}, u32[]{:S(2)}, u32[]{:S(2)}) collective-permute-start(bf16[256,2048]{1,0:T(8,128)(2,1)S(1)} %shard_map.112.mine), channel_id=1, source_target_pairs={{0,24},{8,0},{16,8},{24,16},{1,25},{9,1},{17,9},{25,17},{2,26},{10... | collective-permute-start | bytes 3145736 | tf_op jit(solution)/shard_map/ppermute | solution.py:300
  97.6 15.3 %collective-permute-start.24 = (bf16[256,1024]{1,0:T(8,128)(2,1)S(1)}, bf16[256,1024]{1,0:T(8,128)(2,1)S(1)}, u32[]{:S(2)}, u32[]{:S(2)}) collective-permute-start(bf16[256,1024]{1,0:T(8,128)(2,1)S(1)} %collective-permute-done.23.refs_1_), channel_id=1, source_target_pairs={{0,32},{32,64},{64,96},{96,128},{128,160},{160,192},{192,224},{224... | collective-permute-start | bytes 1572872 | tf_op jit(solution)/shard_map/ppermute | solution.py:300
  98.8 14.1 %collective-permute-start.27 = (bf16[256,1024]{1,0:T(8,128)(2,1)S(1)}, bf16[256,1024]{1,0:T(8,128)(2,1)S(1)}, u32[]{:S(2)}, u32[]{:S(2)}) collective-permute-start(bf16[256,1024]{1,0:T(8,128)(2,1)S(1)} %collective-permute-done.26.refs_2_), channel_id=1, source_target_pairs={{0,224},{32,0},{64,32},{96,64},{128,96},{160,128},{192,160},{224,1... | collective-permute-start | bytes 1572872 | tf_op jit(solution)/shard_map/ppermute | solution.py:300
  112.9 14.3 %collective-permute-start.25 = (bf16[256,1024]{1,0:T(8,128)(2,1)S(1)}, bf16[256,1024]{1,0:T(8,128)(2,1)S(1)}, u32[]{:S(2)}, u32[]{:S(2)}) collective-permute-start(bf16[256,1024]{1,0:T(8,128)(2,1)S(1)} %collective-permute-done.24.refs_3_), channel_id=1, source_target_pairs={{0,32},{32,64},{64,96},{96,128},{128,160},{160,192},{192,224},{224... | collective-permute-start | bytes 1572872 | tf_op jit(solution)/shard_map/ppermute | solution.py:300
  112.9 14.3 %collective-permute-start.28 = (bf16[256,1024]{1,0:T(8,128)(2,1)S(1)}, bf16[256,1024]{1,0:T(8,128)(2,1)S(1)}, u32[]{:S(2)}, u32[]{:S(2)}) collective-permute-start(bf16[256,1024]{1,0:T(8,128)(2,1)S(1)} %collective-permute-done.27.refs_4_), channel_id=1, source_target_pairs={{0,224},{32,0},{64,32},{96,64},{128,96},{160,128},{192,160},{224,1... | collective-permute-start | bytes 1572872 | tf_op jit(solution)/shard_map/ppermute | solution.py:300
  127.3 8.1 %collective-permute-start.29 = (bf16[128,1024]{1,0:T(8,128)(2,1)S(1)}, bf16[128,1024]{1,0:T(8,128)(2,1)S(1)}, u32[]{:S(2)}, u32[]{:S(2)}) collective-permute-start(bf16[128,1024]{1,0:T(8,128)(2,1)S(1)} %get-tuple-element.53), channel_id=1, source_target_pairs={{0,32},{32,64},{64,96},{96,128},{128,160},{160,192},{192,224},{224... | collective-permute-start | bytes 786440 | tf_op jit(solution)/shard_map/ppermute | solution.py:300
  127.6 7.8 %collective-permute-start.30 = (bf16[128,1024]{1,0:T(8,128)(2,1)S(1)}, bf16[128,1024]{1,0:T(8,128)(2,1)S(1)}, u32[]{:S(2)}, u32[]{:S(2)}) collective-permute-start(bf16[128,1024]{1,0:T(8,128)(2,1)S(1)} %get-tuple-element.54), channel_id=1, source_target_pairs={{0,224},{32,0},{64,32},{96,64},{128,96},{160,128},{192,160},{224,1... | collective-permute-start | bytes 786440 | tf_op jit(solution)/shard_map/ppermute | solution.py:300
  136.4 17.3 %collective-permute-start.31 = (bf16[512,1024]{1,0:T(8,128)(2,1)S(1)}, bf16[512,1024]{1,0:T(8,128)(2,1)S(1)}, u32[]{:S(2)}, u32[]{:S(2)}) collective-permute-start(bf16[512,1024]{1,0:T(8,128)(2,1)S(1)} %shard_map.121.hidden), channel_id=1, source_target_pairs={{0,4},{4,0},{1,5},{5,1},{2,6},{6,2},{3,7},{7,3},{8,12},{12,8},{9,1... | collective-permute-start | bytes 3145736 | tf_op jit(solution)/shard_map/ppermute | solution.py:300
  136.5 14.3 %collective-permute-start.32 = (bf16[128,2048]{1,0:T(8,128)(2,1)S(1)}, bf16[128,2048]{1,0:T(8,128)(2,1)S(1)}, u32[]{:S(2)}, u32[]{:S(2)}) collective-permute-start(bf16[128,2048]{1,0:T(8,128)(2,1)S(1)} %get-tuple-element.55), channel_id=1, source_target_pairs={{0,8},{8,16},{16,24},{24,0},{1,9},{9,17},{17,25},{25,1},{2,10},{10... | collective-permute-start | bytes 1572872 | tf_op jit(solution)/shard_map/ppermute | solution.py:300
  137.7 14.0 %collective-permute-start.33 = (bf16[128,2048]{1,0:T(8,128)(2,1)S(1)}, bf16[128,2048]{1,0:T(8,128)(2,1)S(1)}, u32[]{:S(2)}, u32[]{:S(2)}) collective-permute-start(bf16[128,2048]{1,0:T(8,128)(2,1)S(1)} %get-tuple-element.56), channel_id=1, source_target_pairs={{0,24},{8,0},{16,8},{24,16},{1,25},{9,1},{17,9},{25,17},{2,26},{10... | collective-permute-start | bytes 1572872 | tf_op jit(solution)/shard_map/ppermute | solution.py:300
  155.9 9.3 %collective-permute-start.34 = (bf16[64,1024]{1,0:T(8,128)(2,1)S(1)}, bf16[64,1024]{1,0:T(8,128)(2,1)S(1)}, u32[]{:S(2)}, u32[]{:S(2)}) collective-permute-start(bf16[64,1024]{1,0:T(8,128)(2,1)S(1)} %get-tuple-element.58), channel_id=1, source_target_pairs={{0,1},{1,2},{2,3},{3,0},{4,5},{5,6},{6,7},{7,4},{8,9},{9,10},{10,1... | collective-permute-start | bytes 393224 | tf_op jit(solution)/shard_map/ppermute | solution.py:305
  156.0 9.2 %collective-permute-start.35 = (bf16[64,1024]{1,0:T(8,128)(2,1)S(1)}, bf16[64,1024]{1,0:T(8,128)(2,1)S(1)}, u32[]{:S(2)}, u32[]{:S(2)}) collective-permute-start(bf16[64,1024]{1,0:T(8,128)(2,1)S(1)} %get-tuple-element.59), channel_id=1, source_target_pairs={{0,2},{1,3},{2,0},{3,1},{4,6},{5,7},{6,4},{7,5},{8,10},{9,11},{10,... | collective-permute-start | bytes 393224 | tf_op jit(solution)/shard_map/ppermute | solution.py:305
  158.7 6.6 %collective-permute-start.36 = (bf16[64,1024]{1,0:T(8,128)(2,1)S(1)}, bf16[64,1024]{1,0:T(8,128)(2,1)S(1)}, u32[]{:S(2)}, u32[]{:S(2)}) collective-permute-start(bf16[64,1024]{1,0:T(8,128)(2,1)S(1)} %get-tuple-element.60), channel_id=1, source_target_pairs={{0,3},{1,0},{2,1},{3,2},{4,7},{5,4},{6,5},{7,6},{8,11},{9,8},{10,9... | collective-permute-start | bytes 393224 | tf_op jit(solution)/shard_map/ppermute | solution.py:305
  159.2 6.1 %collective-permute-start.37 = (bf16[64,1024]{1,0:T(8,128)(2,1)S(1)}, bf16[64,1024]{1,0:T(8,128)(2,1)S(1)}, u32[]{:S(2)}, u32[]{:S(2)}) collective-permute-start(bf16[64,1024]{1,0:T(8,128)(2,1)S(1)} %get-tuple-element.61), channel_id=1, source_target_pairs={{0,4},{1,5},{2,6},{3,7},{4,0},{5,1},{6,2},{7,3},{8,12},{9,13},{10,... | collective-permute-start | bytes 393224 | tf_op jit(solution)/shard_map/ppermute | solution.py:305
  159.3 7.7 %collective-permute-start.38 = (bf16[64,1024]{1,0:T(8,128)(2,1)S(1)}, bf16[64,1024]{1,0:T(8,128)(2,1)S(1)}, u32[]{:S(2)}, u32[]{:S(2)}) collective-permute-start(bf16[64,1024]{1,0:T(8,128)(2,1)S(1)} %get-tuple-element.62), channel_id=1, source_target_pairs={{0,5},{1,6},{2,7},{3,4},{4,1},{5,2},{6,3},{7,0},{8,13},{9,14},{10,... | collective-permute-start | bytes 393224 | tf_op jit(solution)/shard_map/ppermute | solution.py:305
  165.3 5.9 %collective-permute-start.39 = (bf16[64,1024]{1,0:T(8,128)(2,1)S(1)}, bf16[64,1024]{1,0:T(8,128)(2,1)S(1)}, u32[]{:S(2)}, u32[]{:S(2)}) collective-permute-start(bf16[64,1024]{1,0:T(8,128)(2,1)S(1)} %get-tuple-element.63), channel_id=1, source_target_pairs={{0,6},{1,7},{2,4},{3,5},{4,2},{5,3},{6,0},{7,1},{8,14},{9,15},{10,... | collective-permute-start | bytes 393224 | tf_op jit(solution)/shard_map/ppermute | solution.py:305
  165.3 5.9 %collective-permute-start.40 = (bf16[64,1024]{1,0:T(8,128)(2,1)S(1)}, bf16[64,1024]{1,0:T(8,128)(2,1)S(1)}, u32[]{:S(2)}, u32[]{:S(2)}) collective-permute-start(bf16[64,1024]{1,0:T(8,128)(2,1)S(1)} %get-tuple-element.64), channel_id=1, source_target_pairs={{0,7},{1,4},{2,5},{3,6},{4,3},{5,0},{6,1},{7,2},{8,15},{9,12},{10,... | collective-permute-start | bytes 393224 | tf_op jit(solution)/shard_map/ppermute | solution.py:305
  (3 other events, 31.6 us)
